TPU v7x, 256 devices: a whole 4x4x8 slice. The times are simulated.
256 devices in a mesh: sp: 32 (over z, y), tp: 8 (over x, core).
Axes of the slice: x: 4, y: 4, z: 8, core: 2. Of those that a mesh axis runs over, the one named last changes fastest.
Arguments:
- inputs: bfloat16 [16384, 2048], P('sp', 'tp'), may hold values from -6 to 6
- norm_gain: float32 [2048], replicated, may hold values from 0.1 to 1.9
- latent_query: bfloat16 [2048, 1536], P(None, 'tp'), may hold values from -2 to 2
- latent_down: bfloat16 [2048, 512], replicated, may hold values from -2 to 2
- rope_down: bfloat16 [2048, 32], replicated, may hold values from -2 to 2
- latent_gain: float32 [512], replicated, may hold values from 0.1 to 1.9
- latent_up: bfloat16 [512, 2048], P(None, 'tp'), may hold values from -2 to 2
- window_query: bfloat16 [2048, 1024], P(None, 'tp'), may hold values from -2 to 2
- window_key: bfloat16 [2048, 512], P(None, 'tp'), may hold values from -2 to 2
- window_value: bfloat16 [2048, 512], P(None, 'tp'), may hold values from -0.125 to 0.125
- sink_logit: float32 [16], P('tp'), may hold values from 3 to 8
- out_latent: bfloat16 [1024, 2048], P('tp'), may hold values from -0.1875 to 0.1875
- out_window: bfloat16 [1024, 2048], P('tp'), may hold values from -0.1875 to 0.1875
Outputs:
- attended: bfloat16 [16384, 2048], P('sp', 'tp')
All inputs are finite; a program needn't handle non-finite values.
Results may differ from a plain program's by a relative error of at most 0.017.
Values may be sent and summed in bfloat16 or wider, within the bound.
No kernel may reach another device: no remote copies, remote signals or barrier semaphores. Data moves between devices by JAX's collectives and lax.ppermute only.
A program may use at most 128 MiB of HBM per device.

v0:
```python
import functools
import math

import jax
import jax.numpy as jnp
import numpy as np
from jax import lax
from jax.experimental import pallas as pl
from jax.experimental.pallas import tpu as pltpu
from jax.sharding import Mesh
from jax.sharding import PartitionSpec as P


NOPE = 64
ROPE = 32
HEAD = 64
WINDOW = 128
TILE = 256
epsilon = 1e-06
LOG2E = math.log2(math.e)
LATENT_SCALE = LOG2E * (NOPE + ROPE) ** (-0.5)
WINDOW_SCALE = LOG2E * HEAD ** (-0.5)
GRANT = 12 << 20
PROJECT_GRANT = 60 << 20
UNROLL = 4
SMALLEST = 2.0**-60
LARGEST = 2.0**100
F32 = jnp.float32
BF16 = jnp.bfloat16
VMEM = pltpu.VMEM


NT = (((1,), (1,)), ((), ()))


def dot(a, b):
    return jnp.dot(a, b, preferred_element_type=F32)


def dot_nt(a, b):
    return lax.dot_general(a, b, NT, preferred_element_type=F32)


def rotate(v, cos, sin):
    half = v.shape[0] // 2
    a, b = v[:half], v[half:]
    return jnp.concatenate([a * cos - b * sin, b * cos + a * sin], axis=0)


def params(grant=GRANT):
    return pltpu.CompilerParams(vmem_limit_bytes=grant)


def vmem(count):
    return [pl.BlockSpec(memory_space=VMEM)] * count


SMEM = pl.BlockSpec(memory_space=pltpu.SMEM)
HBM = pl.BlockSpec(memory_space=pltpu.HBM)
ANY = pl.BlockSpec(memory_space=pl.ANY)


def project_kernel(place, gain_ref, lgain_ref, cos_ref, sin_ref, *refs):
    x_hbm, (lq_hbm, rope_hbm, wk_hbm, wv_hbm, wq_hbm, up_hbm, down_hbm), refs = (
        refs[:10],
        refs[10:17],
        refs[17:],
    )
    chunk_refs, (wq_out, wkv_out), refs = refs[:4], refs[4:6], refs[6:]
    xs, hid, rows_ref, wq_ref, up_ref, up_rows, down_ref, sems = refs
    chip, line, core = place[0], place[1], place[2]
    blocks, _, width = xs.shape
    targets = [xs.at[n] for n in range(6)]
    for n in (6, 7):
        targets.insert(len(targets), xs.at[n, 0:TILE])
    for n in (6, 7):
        targets.insert(len(targets), xs.at[n, TILE : 2 * TILE])
    targets += [
        rows_ref.at[0:192],
        rows_ref.at[192:224],
        rows_ref.at[224:288],
        rows_ref.at[288:352],
        wq_ref,
        up_ref,
        down_ref,
    ]
    sources = [*x_hbm, lq_hbm, rope_hbm, wk_hbm, wv_hbm, wq_hbm, up_hbm, down_hbm]
    copies = [
        pltpu.make_async_copy(a, b, sems.at[n]) for n, (a, b) in enumerate(zip(sources, targets))
    ]
    for copy in copies:
        copy.start()
    for copy in copies[:10]:
        copy.wait()

    def normalize(part, carry):
        at = pl.ds(pl.multiple_of(part * TILE, TILE), TILE)
        total = jnp.zeros((TILE, 1), F32)
        for n in range(blocks):
            x = xs[n, at].astype(F32)
            total += jnp.sum(x * x, axis=1, keepdims=True)
        scale = lax.rsqrt(total / (blocks * width) + epsilon)
        for n in range(blocks):
            block = 2 * ((chip + (0, 3, 1, 2)[n // 2]) % 4) + (core + n) % 2
            x = xs[n, at].astype(F32)
            hid[part, :, pl.ds(pl.multiple_of(block * width, width), width)] = (
                x * scale * gain_ref[block]
            ).astype(BF16)
        return carry

    lax.fori_loop(0, 2, normalize, 0)
    for copy in copies[10:]:
        copy.wait()
    rows_ref[352:480] = wq_ref[...].T
    up_rows[...] = up_ref[...].T

    def heads(part, carry):
        at = pl.ds(pl.multiple_of(part * TILE, TILE), TILE)
        hidden = hid[part]
        cos64, sin64 = cos_ref[0:32, at], sin_ref[0:32, at]
        cos32, sin32 = cos_ref[32:48, at], sin_ref[32:48, at]
        raw = dot(hidden, down_ref[...])
        mean = jnp.mean(raw * raw, axis=1, keepdims=True)
        latent = (raw * lax.rsqrt(mean + epsilon) * lgain_ref[...]).astype(BF16)
        together = dot_nt(rows_ref[...], hidden)
        expanded = dot_nt(up_rows[...], latent).astype(BF16)
        queries = together[0:192]
        shared = rotate(together[192:224], cos32, sin32).astype(BF16)
        for h in range(2):
            base = h * (NOPE + ROPE)
            own = h * (NOPE + HEAD)
            plain = queries[base : base + NOPE].astype(BF16)
            turned = rotate(queries[base + NOPE : base + NOPE + ROPE], cos32, sin32).astype(BF16)
            turn = (2 * h + part - line + 4) % 4
            for r, out in enumerate(chunk_refs):

                @pl.when(turn == r)
                def _():
                    out[0:64] = plain
                    out[64:96] = turned
                    out[96:160] = expanded[own : own + NOPE]
                    out[160:192] = shared
                    out[192:256] = expanded[own + NOPE : own + NOPE + HEAD]

        window_q = together[352:480]
        first = rotate(window_q[0:64], cos64, sin64).astype(BF16)
        second = rotate(window_q[64:128], cos64, sin64).astype(BF16)
        for n in range(2):
            cut = slice(n * WINDOW, (n + 1) * WINDOW)
            wq_out[2 * part + n, :, 0:WINDOW] = first[:, cut]
            wq_out[2 * part + n, :, WINDOW : 2 * WINDOW] = second[:, cut]
        wkv_out[0:64, at] = rotate(together[224:288], cos64, sin64).astype(BF16)
        wkv_out[64:128, at] = together[288:352].astype(BF16)
        return carry

    lax.fori_loop(0, 2, heads, 0)


def project(place, small, pieces, weights, rows):
    return pl.pallas_call(
        project_kernel,
        out_shape=[jax.ShapeDtypeStruct((256, TILE), BF16)] * 4
        + [
            jax.ShapeDtypeStruct((rows // WINDOW, 64, 2 * WINDOW), BF16),
            jax.ShapeDtypeStruct((128, rows), BF16),
        ],
        in_specs=[SMEM] + vmem(len(small)) + [HBM] * (len(pieces) + len(weights)),
        out_specs=vmem(6),
        scratch_shapes=[
            VMEM((8, rows, 256), BF16),
            VMEM((2, TILE, 2048), BF16),
            VMEM((480, 2048), BF16),
            VMEM((2048, 128), BF16),
            VMEM((512, 256), BF16),
            VMEM((256, 512), BF16),
            VMEM((2048, 512), BF16),
            pltpu.SemaphoreType.DMA((17,)),
        ],
        compiler_params=params(PROJECT_GRANT),
        cost_estimate=pl.CostEstimate(
            flops=2 * rows * 2048 * 1024, bytes_accessed=8 << 20, transcendentals=0
        ),
        name="project",
    )(place, *small, *pieces, *weights)


def attend_kernel(first, last, tiles, kv_count, unroll, place, *refs):
    q_refs, refs = refs[:tiles], refs[tiles:]
    kv_refs, refs = refs[:kv_count], refs[kv_count:]
    before, refs = (None, refs) if first else (refs[:3], refs[3:])
    if last:
        out_ref, refs = refs[0], refs[1:]
    total, sums, shift, buf, held, queries = refs

    def begin():
        if first:
            total[...] = jnp.zeros_like(total)
            sums[...] = jnp.zeros_like(sums)
            shift[...] = jnp.zeros_like(shift)
        else:
            total[...] = before[0][...]
            sums[...] = before[1][...]
            shift[...] = before[2][...]

    begin()
    inner, _, keys = kv_refs[0].shape
    count = kv_count * inner

    def add(t, p, v):
        sums[t] += p.reshape(keys // 8, 8, TILE).sum(axis=0)
        total[t] += dot(v, p.astype(BF16))

    for n, ref in enumerate(kv_refs):
        held[n * inner : (n + 1) * inner] = ref[...]
    for t in range(tiles):
        buf[0, t] = dot(held[0, 0:96, :].T, q_refs[t][0:96])

    def step(i, carry):
        for b in range(unroll):
            now = unroll * i + b
            k = held[jnp.minimum(now + 1, count - 1), 0:96, :].T
            v = held[now, 96:160, :]
            for t in range(tiles):
                buf[(b + 1) % 2, t] = dot(k, q_refs[t][0:96])
                add(t, jnp.exp2(buf[b % 2, t] * LATENT_SCALE - shift[t]), v)
        return carry

    lax.fori_loop(0, count // unroll, step, 0)

    fits = jnp.max(sums[...]) <= LARGEST
    if first:
        fits = fits & (jnp.min(jnp.sum(sums[...], axis=1)) >= SMALLEST)

    @pl.when(jnp.logical_not(fits))
    def _():
        begin()
        for t in range(tiles):
            queries[t] = q_refs[t][0:96]
        if first:
            shift[...] = jnp.full_like(shift, -jnp.inf)

        def again(n, carry):
            t, b = n // count, n % count
            s = dot(held[b, 0:96, :].T, queries[t]) * LATENT_SCALE
            old = shift[t]
            new = jnp.maximum(old, jnp.max(s, axis=0, keepdims=True))
            shrink = jnp.exp2(old - new)
            sums[t] *= shrink
            total[t] *= shrink
            shift[t] = new
            add(t, jnp.exp2(s - new), held[b, 96:160, :])
            return carry

        lax.fori_loop(0, tiles * count, again, 0)

    if last:
        for t in range(tiles):
            line = (place[3] - t + 4) % 4
            out_ref[line] = (total[t] / jnp.sum(sums[t], axis=0, keepdims=True)).astype(BF16)


def attend(place, chunks, kvs, state=None, last=False, unroll=UNROLL):
    tiles = len(chunks)
    first = state is None
    inner, depth, keys = kvs[0].shape
    holds = [(tiles, HEAD, TILE), (tiles, 8, TILE), (tiles, 1, TILE)]
    spare = [
        VMEM((2, tiles, keys, TILE), F32),
        VMEM((len(kvs) * inner, depth, keys), BF16),
        VMEM((tiles, NOPE + ROPE, TILE), BF16),
    ]
    if last:
        out_shape = [jax.ShapeDtypeStruct((tiles, HEAD, TILE), BF16)]
        spare = [VMEM(s, F32) for s in holds] + spare
    else:
        out_shape = [jax.ShapeDtypeStruct(s, F32) for s in holds]
    args = (*chunks, *kvs) + (() if first else tuple(state))
    work = tiles * TILE * len(kvs) * inner * keys
    return pl.pallas_call(
        functools.partial(attend_kernel, first, last, tiles, len(kvs), unroll),
        out_shape=out_shape,
        in_specs=[SMEM] + vmem(len(args)),
        out_specs=vmem(len(out_shape)),
        scratch_shapes=spare,
        compiler_params=params(),
        cost_estimate=pl.CostEstimate(
            flops=2 * work * 320, bytes_accessed=3 << 20, transcendentals=work
        ),
        name="attend_last" if last else "attend",
    )(place, *args)


def window_kernel(span_ref, q_ref, kv_ref, left_ref, right_ref, sink_ref, out_ref, ext):
    rows = kv_ref.shape[1]
    ext[:, 0:WINDOW] = left_ref[...]
    ext[:, WINDOW : WINDOW + rows] = kv_ref[...]
    ext[:, WINDOW + rows :] = right_ref[...]
    first_span, last_span = span_ref[0] == 0, span_ref[0] == span_ref[1] - 1
    wide = 3 * WINDOW
    key = lax.broadcasted_iota(jnp.int32, (wide, 2 * WINDOW), 0)
    lane = lax.broadcasted_iota(jnp.int32, (wide, 2 * WINDOW), 1)
    offset = key - jnp.where(lane >= WINDOW, lane - WINDOW, lane)
    near = (offset >= 0) & (offset <= 2 * WINDOW)
    side = lax.broadcasted_iota(jnp.int32, (1, 2 * WINDOW), 1)
    sink = jnp.where(side < WINDOW, sink_ref[0], sink_ref[1]) * LOG2E
    blocks = rows // WINDOW
    for n in range(blocks):
        k = ext[0:64, n * WINDOW : n * WINDOW + wide].T
        v = ext[64:128, n * WINDOW : n * WINDOW + wide]
        allowed = near
        if n == 0:
            allowed = allowed & ((key >= WINDOW) | jnp.logical_not(first_span))
        if n == blocks - 1:
            allowed = allowed & ((key < 2 * WINDOW) | jnp.logical_not(last_span))
        s = jnp.where(allowed, dot(k, q_ref[n]) * WINDOW_SCALE, -jnp.inf)
        top = jnp.maximum(jnp.max(s, axis=0, keepdims=True), sink)
        p = jnp.exp2(s - top)
        denom = jnp.sum(p, axis=0, keepdims=True) + jnp.exp2(sink - top)
        o = (dot(v, p.astype(BF16)) / denom).astype(BF16)
        out_ref[0:64, n * WINDOW : (n + 1) * WINDOW] = o[:, 0:WINDOW]
        out_ref[64:128, n * WINDOW : (n + 1) * WINDOW] = o[:, WINDOW:]


def windowed(span, q, kv, left, right, sink):
    smem = pl.BlockSpec(memory_space=pltpu.SMEM)
    vmem = pl.BlockSpec(memory_space=VMEM)
    rows = kv.shape[1]
    return pl.pallas_call(
        window_kernel,
        out_shape=jax.ShapeDtypeStruct((128, rows), BF16),
        in_specs=[smem, vmem, vmem, vmem, vmem, smem],
        out_specs=vmem,
        scratch_shapes=[VMEM((128, rows + 2 * WINDOW), BF16)],
        cost_estimate=pl.CostEstimate(
            flops=rows * 2 * 384 * 256, bytes_accessed=1 << 20, transcendentals=rows * 768
        ),
        compiler_params=params(),
        name="windowed",
    )(span, q, kv, left, right, sink)


def merge_kernel(place, keep_ref, got_ref, win_ref, wl_ref, ww_ref, *refs):
    own_refs, sib_ref, (mixed, lhs) = refs[:4], refs[4], refs[5:]
    sib_refs = [sib_ref.at[k] for k in range(4)]
    chip, core = place[0], place[2]
    for ref, half in ((keep_ref, core), (got_ref, 1 - core)):
        at = pl.ds(pl.multiple_of(half * TILE, TILE), TILE)
        mixed[0:HEAD, at] = ref[0]
        mixed[HEAD : 2 * HEAD, at] = ref[1]
    lhs[:, 0:128] = mixed[...].T
    lhs[:, 128:256] = win_ref[...].T
    rows = lhs[...]
    width = own_refs[0].shape[1]
    for outs, side in ((sib_refs, 1 - core), (own_refs, core)):
        for k in (2, 1, 3, 0):
            start = (2 * ((chip + k) % 4) + side) * width
            at = pl.ds(pl.multiple_of(start, width), width)
            both = jnp.concatenate([wl_ref[:, at], ww_ref[:, at]], axis=0)
            outs[k][...] = dot(rows, both).astype(BF16)


def merge(place, keep, got, win, out_latent, out_window):
    rows = win.shape[1]
    return pl.pallas_call(
        merge_kernel,
        out_shape=[jax.ShapeDtypeStruct((rows, 256), BF16)] * 4
        + [jax.ShapeDtypeStruct((4, rows, 256), BF16)],
        in_specs=[SMEM] + vmem(5),
        out_specs=vmem(5),
        scratch_shapes=[VMEM((128, rows), BF16), VMEM((rows, 256), BF16)],
        compiler_params=params(),
        cost_estimate=pl.CostEstimate(
            flops=2 * rows * 256 * 2048, bytes_accessed=4 << 20, transcendentals=0
        ),
        name="merge",
    )(place, keep, got, win, out_latent, out_window)


SWAP = [(0, 1), (1, 0)]


def shifted(value, axis, by):
    count = lax.axis_size(axis)
    return lax.ppermute(value, axis, [(i, (i + by) % count) for i in range(count)])


def other_core(value):
    return lax.ppermute(value, "c", SWAP)


def ring_step(value):
    count = lax.axis_size("z")
    up = [(2 * i, 2 * ((i + 1) % count)) for i in range(count)]
    down = [(2 * i + 1, 2 * ((i - 1) % count) + 1) for i in range(count)]
    return lax.ppermute(value, ("z", "c"), up + down)


def head_routes(turn):
    routes = []
    for y in range(4):
        d = (y + turn) % 4
        for c in range(2):
            routes.append((2 * y + c, 2 * (2 * c + d // 2) + d % 2))
    return routes


def shards(
    inputs,
    norm_gain,
    latent_query,
    latent_down,
    rope_down,
    latent_gain,
    latent_up,
    window_query,
    window_key,
    window_value,
    sink_logit,
    out_latent,
    out_window,
):
    rows = inputs.shape[0]
    core = lax.axis_index("c")
    line = lax.axis_index("y")
    span = lax.axis_index(("z", "y"))
    spans = lax.axis_size(("z", "y"))
    slot = 2 * (line % 2) + core
    place = jnp.stack([lax.axis_index("x"), line, core, slot]).astype(jnp.int32)

    before = shifted(inputs, "x", 1)
    after = shifted(inputs, "x", -1)
    far_low = shifted(before[:TILE], "x", 1)
    far_high = shifted(after[TILE:], "x", -1)
    pieces = []
    for array in (inputs, before, after, far_low, far_high):
        pieces += [array, other_core(array)]
    powers = np.arange(0, HEAD, 2).astype(np.float64) / HEAD
    inverse = 1.0 / 10000.0**powers
    inverse = jnp.asarray(np.concatenate([inverse, inverse[::2]]), F32)
    positions = (span * rows + jnp.arange(rows)).astype(F32)
    angles = inverse[:, None] * positions[None, :]
    tables = jnp.cos(angles), jnp.sin(angles)
    *chunks, wq, wkv = project(
        place,
        (norm_gain.reshape(8, 1, 256), latent_gain[None], *tables),
        pieces,
        (
            latent_query.T,
            rope_down.T,
            window_key.T,
            window_value.T,
            window_query,
            latent_up,
            latent_down,
        ),
        rows,
    )
    mine = []
    for r, chunk in enumerate(chunks):
        mine.append(lax.ppermute(chunk, ("y", "c"), head_routes(r)))
    left = lax.ppermute(
        wkv[:, rows - WINDOW :], ("z", "y"), [(i, i + 1) for i in range(spans - 1)]
    )
    right = lax.ppermute(
        wkv[:, :WINDOW], ("z", "y"), [(i + 1, i) for i in range(spans - 1)]
    )
    where = jnp.stack([span, spans]).astype(jnp.int32)
    win = windowed(where, wq, wkv, left, right, sink_logit)

    low = jnp.stack([c[96:256] for c in mine])
    high = other_core(low)
    arriving = ring_step(low)
    state = attend(place, mine, [low, high], unroll=2)
    high = ring_step(high)
    low = arriving
    waiting = None
    for n in (1, 2, 3):
        arriving = ring_step(low)
        blocks = [low, other_core(low)]
        if waiting:
            state = attend(place, mine, waiting, state, unroll=2 if n == 2 else UNROLL)
        waiting = [high, other_core(high)]
        if n < 3:
            high = ring_step(high)
        state = attend(place, mine, blocks, state, unroll=2 if n == 1 else UNROLL)
        low = arriving
    blocks = [low, other_core(low)]
    state = attend(place, mine, waiting, state)
    (mixed,) = attend(place, mine, blocks, state, last=True)

    back = lax.all_to_all(mixed, "y", 0, 0, tiled=True)
    pairs = back.reshape(2, 2, HEAD, TILE)
    keep = lax.dynamic_index_in_dim(pairs, core, 0, keepdims=False)
    give = lax.dynamic_index_in_dim(pairs, 1 - core, 0, keepdims=False)
    sums = merge(place, keep, other_core(give), win, out_latent, out_window)
    siblings = other_core(sums[4])
    total = 0
    for k in (2, 1, 3, 0):
        both = sums[k].astype(F32) + siblings[k].astype(F32)
        if k:
            both = shifted(both.astype(BF16), "x", k).astype(F32)
        total = total + both
    return total.astype(BF16)


def solution(mesh):
    shape = (8, 4, 4, 2)
    torus = Mesh(mesh.devices.reshape(shape), ("z", "y", "x", "c"))
    sp, tp = ("z", "y"), ("x", "c")
    in_specs = (
        P(sp, tp),
        P(),
        P(None, tp),
        P(),
        P(),
        P(),
        P(None, tp),
        P(None, tp),
        P(None, tp),
        P(None, tp),
        P(tp),
        P(tp, None),
        P(tp, None),
    )
    return jax.shard_map(
        shards, mesh=torus, in_specs=in_specs, out_specs=P(sp, tp), check_vma=False
    )
```

profile of v0, /device:TPU:1, one launch (start us, length us, event | category | flops | bytes accessed | tf_op | source)
XLA Modules:
  0.0 146.8 jit_solution(9304575241968427417)
XLA Ops:
  0.0 2.0 %collective-permute-start.1 = (bf16[512,256]{1,0:T(8,128)(2,1)}, bf16[512,256]{1,0:T(8,128)(2,1)S(1)}, u32[]{:S(2)}, u32[]{:S(2)}) collective-permute-start(bf16[512,256]{1,0:T(8,128)(2,1)} %refs_0_.1), channel_id=1, source_target_pairs={{0,2},{2,4},{4,6},{6,0},{1,3},{3,5},{5,7},{7,1},{8,10},{10,12},{12... | collective-permute-start | bytes 786440 | tf_op jit(solution)/shard_map/ppermute | solution.py:384
  3.3 4.0 %collective-permute-done.1.refs_2_ = bf16[512,256]{1,0:T(8,128)(2,1)S(1)} collective-permute-done((bf16[512,256]{1,0:T(8,128)(2,1)}, bf16[512,256]{1,0:T(8,128)(2,1)S(1)}, u32[]{:S(2)}, u32[]{:S(2)}) %collective-permute-start.1) | collective-permute-done | bytes 262176 | tf_op jit(solution)/shard_map/ppermute | solution.py:384
  7.3 2.0 %collective-permute-start.5 = (bf16[256,256]{1,0:T(8,128)(2,1)S(1)}, bf16[256,256]{1,0:T(8,128)(2,1)S(1)}, u32[]{:S(2)}, u32[]{:S(2)}) collective-permute-start(bf16[256,256]{1,0:T(8,128)(2,1)S(1)} %slice.48), channel_id=1, source_target_pairs={{0,2},{2,4},{4,6},{6,0},{1,3},{3,5},{5,7},{7,1},{8,10},{10,12},{12... | collective-permute-start | bytes 393224 | tf_op jit(solution)/shard_map/ppermute | solution.py:384
  10.9 3.5 %collective-permute-start = (bf16[512,256]{1,0:T(8,128)(2,1)}, bf16[512,256]{1,0:T(8,128)(2,1)S(1)}, u32[]{:S(2)}, u32[]{:S(2)}) collective-permute-start(bf16[512,256]{1,0:T(8,128)(2,1)} %refs_0_.1), channel_id=1, source_target_pairs={{0,1},{1,0},{2,3},{3,2},{4,5},{5,4},{6,7},{7,6},{8,9},{9,8},{10,11... | collective-permute-start | bytes 786440 | tf_op jit(solution)/shard_map/ppermute | solution.py:388
  14.9 2.3 %collective-permute-start.6 = (bf16[256,256]{1,0:T(8,128)(2,1)S(1)}, bf16[256,256]{1,0:T(8,128)(2,1)S(1)}, u32[]{:S(2)}, u32[]{:S(2)}) collective-permute-start(bf16[256,256]{1,0:T(8,128)(2,1)S(1)} %collective-permute-done.5.refs_6_), channel_id=1, source_target_pairs={{0,1},{1,0},{2,3},{3,2},{4,5},{5,4},{6,7},{7,6},{8,9},{9,8},{10,11... | collective-permute-start | bytes 393224 | tf_op jit(solution)/shard_map/ppermute | solution.py:388
  20.8 7.9 %project.1 = (bf16[256,256]{1,0:T(8,128)(2,1)}, bf16[256,256]{1,0:T(8,128)(2,1)}, bf16[256,256]{1,0:T(8,128)(2,1)}, bf16[256,256]{1,0:T(8,128)(2,1)}, bf16[4,64,...) custom-call(s32[4]{0:T(128)} %pad_add_fusion.place, f32[8,1,256]{2,1,0:T(1,128)} %bitcast.49, f32[1,512]{1,0:T(1,128)} %bitcast.50, ...), custom_call_target="tpu_custom_call" | custom-call | flops 2147483648 | bytes 8388608 | tf_op jit(solution)/shard_map/project/pallas_call | solution.py:160
  28.7 4.6 %collective-permute-start.12 = (bf16[256,256]{1,0:T(8,128)(2,1)}, bf16[256,256]{1,0:T(8,128)(2,1)S(1)}, u32[]{:S(2)}, u32[]{:S(2)}) collective-permute-start(bf16[256,256]{1,0:T(8,128)(2,1)} %get-tuple-element.40), channel_id=1, source_target_pairs={{0,9},{1,25},{8,0},{9,16},{16,1},{17,17},{24,8},{25,24},{2,11},{3,... | collective-permute-start | bytes 393224 | tf_op jit(solution)/shard_map/ppermute | solution.py:460
  36.9 3.4 %collective-permute-start.9 = (bf16[256,256]{1,0:T(8,128)(2,1)}, bf16[256,256]{1,0:T(8,128)(2,1)S(1)}, u32[]{:S(2)}, u32[]{:S(2)}) collective-permute-start(bf16[256,256]{1,0:T(8,128)(2,1)} %get-tuple-element.37), channel_id=1, source_target_pairs={{0,0},{1,16},{8,1},{9,17},{16,8},{17,24},{24,9},{25,25},{2,2},{3,1... | collective-permute-start | bytes 393224 | tf_op jit(solution)/shard_map/ppermute | solution.py:460
  40.4 3.0 %collective-permute-done.9.refs_0_ = bf16[256,256]{1,0:T(8,128)(2,1)S(1)} collective-permute-done((bf16[256,256]{1,0:T(8,128)(2,1)}, bf16[256,256]{1,0:T(8,128)(2,1)S(1)}, u32[]{:S(2)}, u32[]{:S(2)}) %collective-permute-start.9) | collective-permute-done | bytes 131104 | tf_op jit(solution)/shard_map/ppermute | solution.py:460
  43.5 5.7 %collective-permute-start.13 = (bf16[4,160,256]{2,1,0:T(8,128)(2,1)S(1)}, bf16[4,160,256]{2,1,0:T(8,128)(2,1)S(1)}, u32[]{:S(2)}, u32[]{:S(2)}) collective-permute-start(bf16[4,160,256]{2,1,0:T(8,128)(2,1)S(1)} %pad_maximum_fusion.refs_4_), channel_id=1, source_target_pairs={{0,32},{32,64},{64,96},{96,128},{128,160},{160,192},{192,224},{224... | collective-permute-start | bytes 983048 | tf_op jit(solution)/shard_map/ppermute | solution.py:395
  50.7 2.5 %collective-permute-done.13.refs_4_ = bf16[4,160,256]{2,1,0:T(8,128)(2,1)S(1)} collective-permute-done((bf16[4,160,256]{2,1,0:T(8,128)(2,1)S(1)}, bf16[4,160,256]{2,1,0:T(8,128)(2,1)S(1)}, u32[]{:S(2)}, u32[]{:S(2)}) %collective-permute-start.13) | collective-permute-done | bytes 327712 | tf_op jit(solution)/shard_map/ppermute | solution.py:395
  53.2 3.1 %collective-permute-start.14 = (bf16[4,160,256]{2,1,0:T(8,128)(2,1)S(1)}, bf16[4,160,256]{2,1,0:T(8,128)(2,1)S(1)}, u32[]{:S(2)}, u32[]{:S(2)}) collective-permute-start(bf16[4,160,256]{2,1,0:T(8,128)(2,1)S(1)} %collective-permute-done.13.refs_4_), channel_id=1, source_target_pairs={{0,32},{32,64},{64,96},{96,128},{128,160},{160,192},{192,224},{224... | collective-permute-start | bytes 983048 | tf_op jit(solution)/shard_map/ppermute | solution.py:395
  56.7 3.1 %collective-permute-start.20 = (bf16[4,160,256]{2,1,0:T(8,128)(2,1)S(1)}, bf16[4,160,256]{2,1,0:T(8,128)(2,1)S(1)}, u32[]{:S(2)}, u32[]{:S(2)}) collective-permute-start(bf16[4,160,256]{2,1,0:T(8,128)(2,1)S(1)} %collective-permute-done.19.refs_4_), channel_id=1, source_target_pairs={{0,32},{32,64},{64,96},{96,128},{128,160},{160,192},{192,224},{224... | collective-permute-start | bytes 983048 | tf_op jit(solution)/shard_map/ppermute | solution.py:395
  60.3 3.1 %collective-permute-start.15 = (bf16[4,160,256]{2,1,0:T(8,128)(2,1)S(1)}, bf16[4,160,256]{2,1,0:T(8,128)(2,1)S(1)}, u32[]{:S(2)}, u32[]{:S(2)}) collective-permute-start(bf16[4,160,256]{2,1,0:T(8,128)(2,1)S(1)} %collective-permute-done.14.refs_4_), channel_id=1, source_target_pairs={{0,32},{32,64},{64,96},{96,128},{128,160},{160,192},{192,224},{224... | collective-permute-start | bytes 983048 | tf_op jit(solution)/shard_map/ppermute | solution.py:395
  64.0 3.0 %collective-permute-start.21 = (bf16[4,160,256]{2,1,0:T(8,128)(2,1)S(1)}, bf16[4,160,256]{2,1,0:T(8,128)(2,1)S(1)}, u32[]{:S(2)}, u32[]{:S(2)}) collective-permute-start(bf16[4,160,256]{2,1,0:T(8,128)(2,1)S(1)} %collective-permute-done.20.refs_4_), channel_id=1, source_target_pairs={{0,32},{32,64},{64,96},{96,128},{128,160},{160,192},{192,224},{224... | collective-permute-start | bytes 983048 | tf_op jit(solution)/shard_map/ppermute | solution.py:395
  67.0 3.3 %attend.7 = (f32[4,64,256]{2,1,0:T(8,128)S(1)}, f32[4,8,256]{2,1,0:T(8,128)S(1)}, f32[4,1,256]{2,1,0:T(1,128)S(1)}) custom-call(s32[4]{0:T(128)S(1)} %copy-done.1, bf16[256,256]{1,0:T(8,128)(2,1)S(1)} %collective-permute-done.9.refs_0_, bf16[256,256]{1,0:T(8,128)(2,1)S(1)} %collective-permute-done.10.refs_1_, ...), custom_call_target="tpu_custom_call" | custom-call | flops 1342177280 | bytes 3145728 | tf_op jit(solution)/shard_map/attend/pallas_call | solution.py:279
  70.4 2.7 %collective-permute-start.16 = (bf16[4,160,256]{2,1,0:T(8,128)(2,1)S(1)}, bf16[4,160,256]{2,1,0:T(8,128)(2,1)S(1)}, u32[]{:S(2)}, u32[]{:S(2)}) collective-permute-start(bf16[4,160,256]{2,1,0:T(8,128)(2,1)S(1)} %collective-permute-done.15.refs_4_), channel_id=1, source_target_pairs={{0,32},{32,64},{64,96},{96,128},{128,160},{160,192},{192,224},{224... | collective-permute-start | bytes 983048 | tf_op jit(solution)/shard_map/ppermute | solution.py:395
  73.1 3.3 %attend.8 = (f32[4,64,256]{2,1,0:T(8,128)S(1)}, f32[4,8,256]{2,1,0:T(8,128)S(1)}, f32[4,1,256]{2,1,0:T(1,128)S(1)}) custom-call(s32[4]{0:T(128)S(1)} %copy-done.1, bf16[256,256]{1,0:T(8,128)(2,1)S(1)} %collective-permute-done.9.refs_0_, bf16[256,256]{1,0:T(8,128)(2,1)S(1)} %collective-permute-done.10.refs_1_, ...), custom_call_target="tpu_custom_call" | custom-call | flops 1342177280 | bytes 3145728 | tf_op jit(solution)/shard_map/attend/pallas_call | solution.py:279
  76.5 3.3 %attend.9 = (f32[4,64,256]{2,1,0:T(8,128)S(1)}, f32[4,8,256]{2,1,0:T(8,128)S(1)}, f32[4,1,256]{2,1,0:T(1,128)S(1)}) custom-call(s32[4]{0:T(128)S(1)} %copy-done.1, bf16[256,256]{1,0:T(8,128)(2,1)S(1)} %collective-permute-done.9.refs_0_, bf16[256,256]{1,0:T(8,128)(2,1)S(1)} %collective-permute-done.10.refs_1_, ...), custom_call_target="tpu_custom_call" | custom-call | flops 1342177280 | bytes 3145728 | tf_op jit(solution)/shard_map/attend/pallas_call | solution.py:279
  80.4 2.8 %attend.10 = (f32[4,64,256]{2,1,0:T(8,128)S(1)}, f32[4,8,256]{2,1,0:T(8,128)S(1)}, f32[4,1,256]{2,1,0:T(1,128)S(1)}) custom-call(s32[4]{0:T(128)S(1)} %copy-done.1, bf16[256,256]{1,0:T(8,128)(2,1)S(1)} %collective-permute-done.9.refs_0_, bf16[256,256]{1,0:T(8,128)(2,1)S(1)} %collective-permute-done.10.refs_1_, ...), custom_call_target="tpu_custom_call" | custom-call | flops 1342177280 | bytes 3145728 | tf_op jit(solution)/shard_map/attend/pallas_call | solution.py:279
  83.5 2.8 %attend.11 = (f32[4,64,256]{2,1,0:T(8,128)S(1)}, f32[4,8,256]{2,1,0:T(8,128)S(1)}, f32[4,1,256]{2,1,0:T(1,128)S(1)}) custom-call(s32[4]{0:T(128)S(1)} %copy-done.1, bf16[256,256]{1,0:T(8,128)(2,1)S(1)} %collective-permute-done.9.refs_0_, bf16[256,256]{1,0:T(8,128)(2,1)S(1)} %collective-permute-done.10.refs_1_, ...), custom_call_target="tpu_custom_call" | custom-call | flops 1342177280 | bytes 3145728 | tf_op jit(solution)/shard_map/attend/pallas_call | solution.py:279
  86.4 2.8 %attend.12 = (f32[4,64,256]{2,1,0:T(8,128)S(1)}, f32[4,8,256]{2,1,0:T(8,128)S(1)}, f32[4,1,256]{2,1,0:T(1,128)S(1)}) custom-call(s32[4]{0:T(128)S(1)} %copy-done.1, bf16[256,256]{1,0:T(8,128)(2,1)S(1)} %collective-permute-done.9.refs_0_, bf16[256,256]{1,0:T(8,128)(2,1)S(1)} %collective-permute-done.10.refs_1_, ...), custom_call_target="tpu_custom_call" | custom-call | flops 1342177280 | bytes 3145728 | tf_op jit(solution)/shard_map/attend/pallas_call | solution.py:279
  89.2 2.8 %attend.13 = (f32[4,64,256]{2,1,0:T(8,128)S(1)}, f32[4,8,256]{2,1,0:T(8,128)S(1)}, f32[4,1,256]{2,1,0:T(1,128)S(1)}) custom-call(s32[4]{0:T(128)S(1)} %copy-done.1, bf16[256,256]{1,0:T(8,128)(2,1)S(1)} %collective-permute-done.9.refs_0_, bf16[256,256]{1,0:T(8,128)(2,1)S(1)} %collective-permute-done.10.refs_1_, ...), custom_call_target="tpu_custom_call" | custom-call | flops 1342177280 | bytes 3145728 | tf_op jit(solution)/shard_map/attend/pallas_call | solution.py:279
  92.1 3.5 %attend_last.1 = bf16[4,64,256]{2,1,0:T(8,128)(2,1)} custom-call(s32[4]{0:T(128)S(1)} %copy-done.1, bf16[256,256]{1,0:T(8,128)(2,1)S(1)} %collective-permute-done.9.refs_0_, bf16[256,256]{1,0:T(8,128)(2,1)S(1)} %collective-permute-done.10.refs_1_, bf16[256,256]{1,0:T(8,128)(2,1)S(1)} %collective-permute-done.11.refs_2_, ...), custom_call_target="tpu_custom_call" | custom-call | flops 1342177280 | bytes 3145728 | tf_op jit(solution)/shard_map/attend_last/pallas_call | solution.py:279
  95.6 18.1 %all-to-all-start = ((bf16[4,64,256]{2,1,0:T(8,128)(2,1)}), bf16[4,64,256]{2,1,0:T(8,128)(2,1)S(1)}, u32[]{:S(2)}, u32[]{:S(2)}) async-start(bf16[4,64,256]{2,1,0:T(8,128)(2,1)} %attend_last.1), calls=%async_computation | async-start | bytes 262144 | tf_op jit(solution)/shard_map/all_to_all | solution.py:491
  113.7 3.4 %collective-permute-start.29 = (bf16[128,128]{1,0:T(8,128)(2,1)S(1)}, bf16[128,128]{1,0:T(8,128)(2,1)S(1)}, u32[]{:S(2)}, u32[]{:S(2)}) collective-permute-start(bf16[128,128]{1,0:T(8,128)(2,1)S(1)} %get-tuple-element.73), channel_id=1, source_target_pairs={{0,8},{8,16},{16,24},{24,32},{32,40},{40,48},{48,56},{56,64},{64,7... | collective-permute-start | bytes 98312 | tf_op jit(solution)/shard_map/ppermute | solution.py:461
  121.8 2.0 %windowed.1.win_ref = bf16[128,512]{1,0:T(8,128)(2,1)S(1)} custom-call(s32[2]{0:T(128)S(1)} %pad_add_fusion.1.span_ref, bf16[4,64,256]{2,1,0:T(8,128)(2,1)S(1)} %copy-done.5, bf16[128,512]{1,0:T(8,128)(2,1)S(1)} %copy-done, bf16[128,128]{1,0:T(8,128)(2,1)S(1)} %collective-permute-done.29.left_ref, bf16[128,128]{1,0:T(8,128)(2,1)S(1)} %collective-permute-done.30.right_ref, ...), custom_call_target="tpu_custom_call" | custom-call | flops 100663296 | bytes 1048576 | tf_op jit(solution)/shard_map/windowed/pallas_call | solution.py:328
  125.2 2.5 %collective-permute-start.31 = (bf16[4,512,256]{2,1,0:T(8,128)(2,1)S(1)}, bf16[4,512,256]{2,1,0:T(8,128)(2,1)S(1)}, u32[]{:S(2)}, u32[]{:S(2)}) collective-permute-start(bf16[4,512,256]{2,1,0:T(8,128)(2,1)S(1)} %get-tuple-element.65), channel_id=1, source_target_pairs={{0,1},{1,0},{2,3},{3,2},{4,5},{5,4},{6,7},{7,6},{8,9},{9,8},{10,11... | collective-permute-start | bytes 3145736 | tf_op jit(solution)/shard_map/ppermute | solution.py:388
  127.7 2.3 %collective-permute-done.31 = bf16[4,512,256]{2,1,0:T(8,128)(2,1)S(1)} collective-permute-done((bf16[4,512,256]{2,1,0:T(8,128)(2,1)S(1)}, bf16[4,512,256]{2,1,0:T(8,128)(2,1)S(1)}, u32[]{:S(2)}, u32[]{:S(2)}) %collective-permute-start.31) | collective-permute-done | bytes 1048608 | tf_op jit(solution)/shard_map/ppermute | solution.py:388
  132.2 2.0 %collective-permute-start.33 = (bf16[512,256]{1,0:T(8,128)(2,1)S(1)}, bf16[512,256]{1,0:T(8,128)(2,1)S(1)}, u32[]{:S(2)}, u32[]{:S(2)}) collective-permute-start(bf16[512,256]{1,0:T(8,128)(2,1)S(1)} %get-tuple-element.71), channel_id=1, source_target_pairs={{0,2},{2,4},{4,6},{6,0},{1,3},{3,5},{5,7},{7,1},{8,10},{10,12},{12... | collective-permute-start | bytes 786440 | tf_op jit(solution)/shard_map/ppermute | solution.py:384
  134.9 4.5 %collective-permute-done.32 = bf16[512,256]{1,0:T(8,128)(2,1)S(1)} collective-permute-done((bf16[512,256]{1,0:T(8,128)(2,1)S(1)}, bf16[512,256]{1,0:T(8,128)(2,1)S(1)}, u32[]{:S(2)}, u32[]{:S(2)}) %collective-permute-start.32) | collective-permute-done | bytes 262176 | tf_op jit(solution)/shard_map/ppermute | solution.py:384
  139.3 6.3 %collective-permute-done.33 = bf16[512,256]{1,0:T(8,128)(2,1)S(1)} collective-permute-done((bf16[512,256]{1,0:T(8,128)(2,1)S(1)}, bf16[512,256]{1,0:T(8,128)(2,1)S(1)}, u32[]{:S(2)}, u32[]{:S(2)}) %collective-permute-start.33) | collective-permute-done | bytes 262176 | tf_op jit(solution)/shard_map/ppermute | solution.py:384
  (96 shorter events, 24.6 us)
Async XLA Ops:
  0.0 7.3 %collective-permute-start.1 = (bf16[512,256]{1,0:T(8,128)(2,1)}, bf16[512,256]{1,0:T(8,128)(2,1)S(1)}, u32[]{:S(2)}, u32[]{:S(2)}) collective-permute-start(bf16[512,256]{1,0:T(8,128)(2,1)} %refs_0_.1), channel_id=1, source_target_pairs={{0,2},{2,4},{4,6},{6,0},{1,3},{3,5},{5,7},{7,1},{8,10},{10,12},{12... | collective-permute-start | bytes 786440 | tf_op jit(solution)/shard_map/ppermute | solution.py:384
  2.0 7.3 %collective-permute-start.3 = (bf16[512,256]{1,0:T(8,128)(2,1)}, bf16[512,256]{1,0:T(8,128)(2,1)S(1)}, u32[]{:S(2)}, u32[]{:S(2)}) collective-permute-start(bf16[512,256]{1,0:T(8,128)(2,1)} %refs_0_.1), channel_id=1, source_target_pairs={{0,6},{2,0},{4,2},{6,4},{1,7},{3,1},{5,3},{7,5},{8,14},{10,8},{12,... | collective-permute-start | bytes 786440 | tf_op jit(solution)/shard_map/ppermute | solution.py:384
  7.3 7.7 %collective-permute-start.5 = (bf16[256,256]{1,0:T(8,128)(2,1)S(1)}, bf16[256,256]{1,0:T(8,128)(2,1)S(1)}, u32[]{:S(2)}, u32[]{:S(2)}) collective-permute-start(bf16[256,256]{1,0:T(8,128)(2,1)S(1)} %slice.48), channel_id=1, source_target_pairs={{0,2},{2,4},{4,6},{6,0},{1,3},{3,5},{5,7},{7,1},{8,10},{10,12},{12... | collective-permute-start | bytes 393224 | tf_op jit(solution)/shard_map/ppermute | solution.py:384
  9.3 7.9 %collective-permute-start.7 = (bf16[256,256]{1,0:T(8,128)(2,1)S(1)}, bf16[256,256]{1,0:T(8,128)(2,1)S(1)}, u32[]{:S(2)}, u32[]{:S(2)}) collective-permute-start(bf16[256,256]{1,0:T(8,128)(2,1)S(1)} %slice.49), channel_id=1, source_target_pairs={{0,6},{2,0},{4,2},{6,4},{1,7},{3,1},{5,3},{7,5},{8,14},{10,8},{12,... | collective-permute-start | bytes 393224 | tf_op jit(solution)/shard_map/ppermute | solution.py:384
  10.9 8.9 %collective-permute-start = (bf16[512,256]{1,0:T(8,128)(2,1)}, bf16[512,256]{1,0:T(8,128)(2,1)S(1)}, u32[]{:S(2)}, u32[]{:S(2)}) collective-permute-start(bf16[512,256]{1,0:T(8,128)(2,1)} %refs_0_.1), channel_id=1, source_target_pairs={{0,1},{1,0},{2,3},{3,2},{4,5},{5,4},{6,7},{7,6},{8,9},{9,8},{10,11... | collective-permute-start | bytes 786440 | tf_op jit(solution)/shard_map/ppermute | solution.py:388
  14.4 5.4 %collective-permute-start.2 = (bf16[512,256]{1,0:T(8,128)(2,1)S(1)}, bf16[512,256]{1,0:T(8,128)(2,1)S(1)}, u32[]{:S(2)}, u32[]{:S(2)}) collective-permute-start(bf16[512,256]{1,0:T(8,128)(2,1)S(1)} %collective-permute-done.1.refs_2_), channel_id=1, source_target_pairs={{0,1},{1,0},{2,3},{3,2},{4,5},{5,4},{6,7},{7,6},{8,9},{9,8},{10,11... | collective-permute-start | bytes 786440 | tf_op jit(solution)/shard_map/ppermute | solution.py:388
  14.4 5.4 %collective-permute-start.4 = (bf16[512,256]{1,0:T(8,128)(2,1)S(1)}, bf16[512,256]{1,0:T(8,128)(2,1)S(1)}, u32[]{:S(2)}, u32[]{:S(2)}) collective-permute-start(bf16[512,256]{1,0:T(8,128)(2,1)S(1)} %collective-permute-done.3.refs_4_), channel_id=1, source_target_pairs={{0,1},{1,0},{2,3},{3,2},{4,5},{5,4},{6,7},{7,6},{8,9},{9,8},{10,11... | collective-permute-start | bytes 786440 | tf_op jit(solution)/shard_map/ppermute | solution.py:388
  28.7 11.6 %collective-permute-start.12 = (bf16[256,256]{1,0:T(8,128)(2,1)}, bf16[256,256]{1,0:T(8,128)(2,1)S(1)}, u32[]{:S(2)}, u32[]{:S(2)}) collective-permute-start(bf16[256,256]{1,0:T(8,128)(2,1)} %get-tuple-element.40), channel_id=1, source_target_pairs={{0,9},{1,25},{8,0},{9,16},{16,1},{17,17},{24,8},{25,24},{2,11},{3,... | collective-permute-start | bytes 393224 | tf_op jit(solution)/shard_map/ppermute | solution.py:460
  33.3 7.0 %collective-permute-start.11 = (bf16[256,256]{1,0:T(8,128)(2,1)}, bf16[256,256]{1,0:T(8,128)(2,1)S(1)}, u32[]{:S(2)}, u32[]{:S(2)}) collective-permute-start(bf16[256,256]{1,0:T(8,128)(2,1)} %get-tuple-element.39), channel_id=1, source_target_pairs={{0,8},{1,24},{8,9},{9,25},{16,0},{17,16},{24,1},{25,17},{2,10},{3,... | collective-permute-start | bytes 393224 | tf_op jit(solution)/shard_map/ppermute | solution.py:460
  35.0 5.4 %collective-permute-start.10 = (bf16[256,256]{1,0:T(8,128)(2,1)}, bf16[256,256]{1,0:T(8,128)(2,1)S(1)}, u32[]{:S(2)}, u32[]{:S(2)}) collective-permute-start(bf16[256,256]{1,0:T(8,128)(2,1)} %get-tuple-element.38), channel_id=1, source_target_pairs={{0,1},{1,17},{8,8},{9,24},{16,9},{17,25},{24,0},{25,16},{2,3},{3,1... | collective-permute-start | bytes 393224 | tf_op jit(solution)/shard_map/ppermute | solution.py:460
  36.9 6.5 %collective-permute-start.9 = (bf16[256,256]{1,0:T(8,128)(2,1)}, bf16[256,256]{1,0:T(8,128)(2,1)S(1)}, u32[]{:S(2)}, u32[]{:S(2)}) collective-permute-start(bf16[256,256]{1,0:T(8,128)(2,1)} %get-tuple-element.37), channel_id=1, source_target_pairs={{0,0},{1,16},{8,1},{9,17},{16,8},{17,24},{24,9},{25,25},{2,2},{3,1... | collective-permute-start | bytes 393224 | tf_op jit(solution)/shard_map/ppermute | solution.py:460
  43.4 5.8 %collective-permute-start.18 = (bf16[4,160,256]{2,1,0:T(8,128)(2,1)S(1)}, bf16[4,160,256]{2,1,0:T(8,128)(2,1)S(1)}, u32[]{:S(2)}, u32[]{:S(2)}) collective-permute-start(bf16[4,160,256]{2,1,0:T(8,128)(2,1)S(1)} %pad_maximum_fusion.refs_4_), channel_id=1, source_target_pairs={{0,1},{1,0},{2,3},{3,2},{4,5},{5,4},{6,7},{7,6},{8,9},{9,8},{10,11... | collective-permute-start | bytes 983048 | tf_op jit(solution)/shard_map/ppermute | solution.py:388
  43.5 9.7 %collective-permute-start.13 = (bf16[4,160,256]{2,1,0:T(8,128)(2,1)S(1)}, bf16[4,160,256]{2,1,0:T(8,128)(2,1)S(1)}, u32[]{:S(2)}, u32[]{:S(2)}) collective-permute-start(bf16[4,160,256]{2,1,0:T(8,128)(2,1)S(1)} %pad_maximum_fusion.refs_4_), channel_id=1, source_target_pairs={{0,32},{32,64},{64,96},{96,128},{128,160},{160,192},{192,224},{224... | collective-permute-start | bytes 983048 | tf_op jit(solution)/shard_map/ppermute | solution.py:395
  49.2 7.5 %collective-permute-start.19 = (bf16[4,160,256]{2,1,0:T(8,128)(2,1)S(1)}, bf16[4,160,256]{2,1,0:T(8,128)(2,1)S(1)}, u32[]{:S(2)}, u32[]{:S(2)}) collective-permute-start(bf16[4,160,256]{2,1,0:T(8,128)(2,1)S(1)} %collective-permute-done.18.refs_5_), channel_id=1, source_target_pairs={{0,32},{32,64},{64,96},{96,128},{128,160},{160,192},{192,224},{224... | collective-permute-start | bytes 983048 | tf_op jit(solution)/shard_map/ppermute | solution.py:395
  53.2 7.1 %collective-permute-start.14 = (bf16[4,160,256]{2,1,0:T(8,128)(2,1)S(1)}, bf16[4,160,256]{2,1,0:T(8,128)(2,1)S(1)}, u32[]{:S(2)}, u32[]{:S(2)}) collective-permute-start(bf16[4,160,256]{2,1,0:T(8,128)(2,1)S(1)} %collective-permute-done.13.refs_4_), channel_id=1, source_target_pairs={{0,32},{32,64},{64,96},{96,128},{128,160},{160,192},{192,224},{224... | collective-permute-start | bytes 983048 | tf_op jit(solution)/shard_map/ppermute | solution.py:395
  56.7 7.3 %collective-permute-start.20 = (bf16[4,160,256]{2,1,0:T(8,128)(2,1)S(1)}, bf16[4,160,256]{2,1,0:T(8,128)(2,1)S(1)}, u32[]{:S(2)}, u32[]{:S(2)}) collective-permute-start(bf16[4,160,256]{2,1,0:T(8,128)(2,1)S(1)} %collective-permute-done.19.refs_4_), channel_id=1, source_target_pairs={{0,32},{32,64},{64,96},{96,128},{128,160},{160,192},{192,224},{224... | collective-permute-start | bytes 983048 | tf_op jit(solution)/shard_map/ppermute | solution.py:395
  59.8 10.4 %collective-permute-start.27 = (bf16[4,160,256]{2,1,0:T(8,128)(2,1)S(1)}, bf16[4,160,256]{2,1,0:T(8,128)(2,1)S(1)}, u32[]{:S(2)}, u32[]{:S(2)}) collective-permute-start(bf16[4,160,256]{2,1,0:T(8,128)(2,1)S(1)} %collective-permute-done.13.refs_4_), channel_id=1, source_target_pairs={{0,1},{1,0},{2,3},{3,2},{4,5},{5,4},{6,7},{7,6},{8,9},{9,8},{10,11... | collective-permute-start | bytes 983048 | tf_op jit(solution)/shard_map/ppermute | solution.py:388
  60.3 10.0 %collective-permute-start.15 = (bf16[4,160,256]{2,1,0:T(8,128)(2,1)S(1)}, bf16[4,160,256]{2,1,0:T(8,128)(2,1)S(1)}, u32[]{:S(2)}, u32[]{:S(2)}) collective-permute-start(bf16[4,160,256]{2,1,0:T(8,128)(2,1)S(1)} %collective-permute-done.14.refs_4_), channel_id=1, source_target_pairs={{0,32},{32,64},{64,96},{96,128},{128,160},{160,192},{192,224},{224... | collective-permute-start | bytes 983048 | tf_op jit(solution)/shard_map/ppermute | solution.py:395
  63.5 12.9 %collective-permute-start.26 = (bf16[4,160,256]{2,1,0:T(8,128)(2,1)S(1)}, bf16[4,160,256]{2,1,0:T(8,128)(2,1)S(1)}, u32[]{:S(2)}, u32[]{:S(2)}) collective-permute-start(bf16[4,160,256]{2,1,0:T(8,128)(2,1)S(1)} %collective-permute-done.19.refs_4_), channel_id=1, source_target_pairs={{0,1},{1,0},{2,3},{3,2},{4,5},{5,4},{6,7},{7,6},{8,9},{9,8},{10,11... | collective-permute-start | bytes 983048 | tf_op jit(solution)/shard_map/ppermute | solution.py:388
  63.5 16.9 %collective-permute-start.25 = (bf16[4,160,256]{2,1,0:T(8,128)(2,1)S(1)}, bf16[4,160,256]{2,1,0:T(8,128)(2,1)S(1)}, u32[]{:S(2)}, u32[]{:S(2)}) collective-permute-start(bf16[4,160,256]{2,1,0:T(8,128)(2,1)S(1)} %collective-permute-done.14.refs_4_), channel_id=1, source_target_pairs={{0,1},{1,0},{2,3},{3,2},{4,5},{5,4},{6,7},{7,6},{8,9},{9,8},{10,11... | collective-permute-start | bytes 983048 | tf_op jit(solution)/shard_map/ppermute | solution.py:388
  64.0 15.8 %collective-permute-start.21 = (bf16[4,160,256]{2,1,0:T(8,128)(2,1)S(1)}, bf16[4,160,256]{2,1,0:T(8,128)(2,1)S(1)}, u32[]{:S(2)}, u32[]{:S(2)}) collective-permute-start(bf16[4,160,256]{2,1,0:T(8,128)(2,1)S(1)} %collective-permute-done.20.refs_4_), channel_id=1, source_target_pairs={{0,32},{32,64},{64,96},{96,128},{128,160},{160,192},{192,224},{224... | collective-permute-start | bytes 983048 | tf_op jit(solution)/shard_map/ppermute | solution.py:395
  70.3 13.2 %collective-permute-start.24 = (bf16[4,160,256]{2,1,0:T(8,128)(2,1)S(1)}, bf16[4,160,256]{2,1,0:T(8,128)(2,1)S(1)}, u32[]{:S(2)}, u32[]{:S(2)}) collective-permute-start(bf16[4,160,256]{2,1,0:T(8,128)(2,1)S(1)} %collective-permute-done.20.refs_4_), channel_id=1, source_target_pairs={{0,1},{1,0},{2,3},{3,2},{4,5},{5,4},{6,7},{7,6},{8,9},{9,8},{10,11... | collective-permute-start | bytes 983048 | tf_op jit(solution)/shard_map/ppermute | solution.py:388
  70.4 12.8 %collective-permute-start.16 = (bf16[4,160,256]{2,1,0:T(8,128)(2,1)S(1)}, bf16[4,160,256]{2,1,0:T(8,128)(2,1)S(1)}, u32[]{:S(2)}, u32[]{:S(2)}) collective-permute-start(bf16[4,160,256]{2,1,0:T(8,128)(2,1)S(1)} %collective-permute-done.15.refs_4_), channel_id=1, source_target_pairs={{0,32},{32,64},{64,96},{96,128},{128,160},{160,192},{192,224},{224... | collective-permute-start | bytes 983048 | tf_op jit(solution)/shard_map/ppermute | solution.py:395
  76.4 10.0 %collective-permute-start.23 = (bf16[4,160,256]{2,1,0:T(8,128)(2,1)S(1)}, bf16[4,160,256]{2,1,0:T(8,128)(2,1)S(1)}, u32[]{:S(2)}, u32[]{:S(2)}) collective-permute-start(bf16[4,160,256]{2,1,0:T(8,128)(2,1)S(1)} %collective-permute-done.15.refs_4_), channel_id=1, source_target_pairs={{0,1},{1,0},{2,3},{3,2},{4,5},{5,4},{6,7},{7,6},{8,9},{9,8},{10,11... | collective-permute-start | bytes 983048 | tf_op jit(solution)/shard_map/ppermute | solution.py:388
  79.8 9.4 %collective-permute-start.22 = (bf16[4,160,256]{2,1,0:T(8,128)(2,1)S(1)}, bf16[4,160,256]{2,1,0:T(8,128)(2,1)S(1)}, u32[]{:S(2)}, u32[]{:S(2)}) collective-permute-start(bf16[4,160,256]{2,1,0:T(8,128)(2,1)S(1)} %collective-permute-done.21.refs_4_), channel_id=1, source_target_pairs={{0,1},{1,0},{2,3},{3,2},{4,5},{5,4},{6,7},{7,6},{8,9},{9,8},{10,11... | collective-permute-start | bytes 983048 | tf_op jit(solution)/shard_map/ppermute | solution.py:388
  83.2 8.8 %collective-permute-start.17 = (bf16[4,160,256]{2,1,0:T(8,128)(2,1)S(1)}, bf16[4,160,256]{2,1,0:T(8,128)(2,1)S(1)}, u32[]{:S(2)}, u32[]{:S(2)}) collective-permute-start(bf16[4,160,256]{2,1,0:T(8,128)(2,1)S(1)} %collective-permute-done.16.refs_4_), channel_id=1, source_target_pairs={{0,1},{1,0},{2,3},{3,2},{4,5},{5,4},{6,7},{7,6},{8,9},{9,8},{10,11... | collective-permute-start | bytes 983048 | tf_op jit(solution)/shard_map/ppermute | solution.py:388
  95.6 22.9 %all-to-all-start = ((bf16[4,64,256]{2,1,0:T(8,128)(2,1)}), bf16[4,64,256]{2,1,0:T(8,128)(2,1)S(1)}, u32[]{:S(2)}, u32[]{:S(2)}) async-start(bf16[4,64,256]{2,1,0:T(8,128)(2,1)} %attend_last.1), calls=%async_computation | async-start | bytes 262144 | tf_op jit(solution)/shard_map/all_to_all | solution.py:491
  113.7 6.9 %collective-permute-start.29 = (bf16[128,128]{1,0:T(8,128)(2,1)S(1)}, bf16[128,128]{1,0:T(8,128)(2,1)S(1)}, u32[]{:S(2)}, u32[]{:S(2)}) collective-permute-start(bf16[128,128]{1,0:T(8,128)(2,1)S(1)} %get-tuple-element.73), channel_id=1, source_target_pairs={{0,8},{8,16},{16,24},{24,32},{32,40},{40,48},{48,56},{56,64},{64,7... | collective-permute-start | bytes 98312 | tf_op jit(solution)/shard_map/ppermute | solution.py:461
  118.5 5.3 %collective-permute-start.28 = (bf16[2,64,256]{2,1,0:T(8,128)(2,1)S(1)}, bf16[2,64,256]{2,1,0:T(8,128)(2,1)S(1)}, u32[]{:S(2)}, u32[]{:S(2)}) collective-permute-start(bf16[2,64,256]{2,1,0:T(8,128)(2,1)S(1)} %get-tuple-element.74), channel_id=1, source_target_pairs={{0,1},{1,0},{2,3},{3,2},{4,5},{5,4},{6,7},{7,6},{8,9},{9,8},{10,11... | collective-permute-start | bytes 196616 | tf_op jit(solution)/shard_map/ppermute | solution.py:388
  130.2 9.1 %collective-permute-start.32 = (bf16[512,256]{1,0:T(8,128)(2,1)S(1)}, bf16[512,256]{1,0:T(8,128)(2,1)S(1)}, u32[]{:S(2)}, u32[]{:S(2)}) collective-permute-start(bf16[512,256]{1,0:T(8,128)(2,1)S(1)} %get-tuple-element.69), channel_id=1, source_target_pairs={{0,4},{2,6},{4,0},{6,2},{1,5},{3,7},{5,1},{7,3},{8,12},{10,14},{12... | collective-permute-start | bytes 786440 | tf_op jit(solution)/shard_map/ppermute | solution.py:384
  132.2 13.5 %collective-permute-start.33 = (bf16[512,256]{1,0:T(8,128)(2,1)S(1)}, bf16[512,256]{1,0:T(8,128)(2,1)S(1)}, u32[]{:S(2)}, u32[]{:S(2)}) collective-permute-start(bf16[512,256]{1,0:T(8,128)(2,1)S(1)} %get-tuple-element.71), channel_id=1, source_target_pairs={{0,2},{2,4},{4,6},{6,0},{1,3},{3,5},{5,7},{7,1},{8,10},{10,12},{12... | collective-permute-start | bytes 786440 | tf_op jit(solution)/shard_map/ppermute | solution.py:384
  134.2 11.7 %collective-permute-start.34 = (bf16[512,256]{1,0:T(8,128)(2,1)S(1)}, bf16[512,256]{1,0:T(8,128)(2,1)S(1)}, u32[]{:S(2)}, u32[]{:S(2)}) collective-permute-start(bf16[512,256]{1,0:T(8,128)(2,1)S(1)} %get-tuple-element.70), channel_id=1, source_target_pairs={{0,6},{2,0},{4,2},{6,4},{1,7},{3,1},{5,3},{7,5},{8,14},{10,8},{12,... | collective-permute-start | bytes 786440 | tf_op jit(solution)/shard_map/ppermute | solution.py:384
  (19 other events, 242.5 us)
where the time goes:
time: 148 us; the launch traced here: 147 us
  starting transfers between devices  80.8 us (55%)
  Pallas kernels  35.9 us (24%)
  waiting for transfers between devices  25 us (17%)
  other arithmetic  3.63 us (2%)
    pallas_call x8, Pallas kernels, attend(): pl.pallas_call(functools.partial(attend_kernel, first, last, tiles, len(k...  24.6 us
    ppermute x7, starting transfers between devices, ring_step(): return lax.ppermute(value, ('z', 'c'), up + down)  22.2 us
    all_to_all x1, starting transfers between devices, shards(): back = lax.all_to_all(mixed, 'y', 0, 0, tiled=True)  18.1 us
    ppermute x7, waiting for transfers between devices, shifted(): lax.ppermute(value, axis, [(i, (i + by) % count) for i in range(count)])  15 us
    ppermute x15, starting transfers between devices, other_core(): return lax.ppermute(value, 'c', SWAP)  12.7 us
    ppermute x7, starting transfers between devices, shifted(): lax.ppermute(value, axis, [(i, (i + by) % count) for i in range(count)])  11.6 us
    ppermute x4, starting transfers between devices, shards(): mine.append(lax.ppermute(chunk, ('y', 'c'), head_routes(r)))  11.5 us
    pallas_call x1, Pallas kernels, project(): pl.pallas_call(project_kernel, out_shape=[jax.ShapeDtypeStruct((256, TILE...  7.95 us
  transfers between devices with their start and end apart: 36, of which 11 were waited for; matrix products, arithmetic and copies ran while one was open for 2% of the time, Pallas kernels for 16%

commit v1 on v0

--- a/solution.py
+++ b/solution.py
@@ -66,7 +66,7 @@
         refs[10:17],
         refs[17:],
     )
-    chunk_refs, (wq_out, wkv_out), refs = refs[:4], refs[4:6], refs[6:]
+    chunk_refs, (wq_out, wkv_out), refs = refs[:2], refs[2:4], refs[4:]
     xs, hid, rows_ref, wq_ref, up_ref, up_rows, down_ref, sems = refs
     chip, line, core = place[0], place[1], place[2]
     blocks, _, width = xs.shape
@@ -131,16 +131,16 @@
             own = h * (NOPE + HEAD)
             plain = queries[base : base + NOPE].astype(BF16)
             turned = rotate(queries[base + NOPE : base + NOPE + ROPE], cos32, sin32).astype(BF16)
-            turn = (2 * h + part - line + 4) % 4
+            turn = (h + line) % 2
             for r, out in enumerate(chunk_refs):
 
                 @pl.when(turn == r)
                 def _():
-                    out[0:64] = plain
-                    out[64:96] = turned
-                    out[96:160] = expanded[own : own + NOPE]
-                    out[160:192] = shared
-                    out[192:256] = expanded[own + NOPE : own + NOPE + HEAD]
+                    out[part, 0:64] = plain
+                    out[part, 64:96] = turned
+                    out[part, 96:160] = expanded[own : own + NOPE]
+                    out[part, 160:192] = shared
+                    out[part, 192:256] = expanded[own + NOPE : own + NOPE + HEAD]
 
         window_q = together[352:480]
         first = rotate(window_q[0:64], cos64, sin64).astype(BF16)
@@ -159,13 +159,13 @@
 def project(place, small, pieces, weights, rows):
     return pl.pallas_call(
         project_kernel,
-        out_shape=[jax.ShapeDtypeStruct((256, TILE), BF16)] * 4
+        out_shape=[jax.ShapeDtypeStruct((2, 256, TILE), BF16)] * 2
         + [
             jax.ShapeDtypeStruct((rows // WINDOW, 64, 2 * WINDOW), BF16),
             jax.ShapeDtypeStruct((128, rows), BF16),
         ],
         in_specs=[SMEM] + vmem(len(small)) + [HBM] * (len(pieces) + len(weights)),
-        out_specs=vmem(6),
+        out_specs=vmem(4),
         scratch_shapes=[
             VMEM((8, rows, 256), BF16),
             VMEM((2, TILE, 2048), BF16),
@@ -185,7 +185,7 @@
 
 
 def attend_kernel(first, last, tiles, kv_count, unroll, place, *refs):
-    q_refs, refs = refs[:tiles], refs[tiles:]
+    q_refs, refs = [refs[t // 2].at[t % 2] for t in range(tiles)], refs[tiles // 2 :]
     kv_refs, refs = refs[:kv_count], refs[kv_count:]
     before, refs = (None, refs) if first else (refs[:3], refs[3:])
     if last:
@@ -255,12 +255,12 @@
 
     if last:
         for t in range(tiles):
-            line = (place[3] - t + 4) % 4
+            line = 2 * ((place[2] + t // 2) % 2) + (place[1] + t) % 2
             out_ref[line] = (total[t] / jnp.sum(sums[t], axis=0, keepdims=True)).astype(BF16)
 
 
 def attend(place, chunks, kvs, state=None, last=False, unroll=UNROLL):
-    tiles = len(chunks)
+    tiles = 2 * len(chunks)
     first = state is None
     inner, depth, keys = kvs[0].shape
     holds = [(tiles, HEAD, TILE), (tiles, 8, TILE), (tiles, 1, TILE)]
@@ -396,12 +396,9 @@
 
 
 def head_routes(turn):
-    routes = []
-    for y in range(4):
-        d = (y + turn) % 4
-        for c in range(2):
-            routes.append((2 * y + c, 2 * (2 * c + d // 2) + d % 2))
-    return routes
+    return [
+        (2 * y + c, 2 * (2 * c + (y + turn) % 2) + y // 2) for y in range(4) for c in range(2)
+    ]
 
 
 def shards(
@@ -455,9 +452,12 @@
         ),
         rows,
     )
-    mine = []
+    arrived = []
     for r, chunk in enumerate(chunks):
-        mine.append(lax.ppermute(chunk, ("y", "c"), head_routes(r)))
+        arrived.append(lax.ppermute(chunk, ("y", "c"), head_routes(r)))
+    kept = jnp.stack([lax.dynamic_index_in_dim(a, core, 0, keepdims=False) for a in arrived])
+    given = jnp.stack([lax.dynamic_index_in_dim(a, 1 - core, 0, keepdims=False) for a in arrived])
+    mine = [kept, other_core(given)]
     left = lax.ppermute(
         wkv[:, rows - WINDOW :], ("z", "y"), [(i, i + 1) for i in range(spans - 1)]
     )
@@ -467,7 +467,7 @@
     where = jnp.stack([span, spans]).astype(jnp.int32)
     win = windowed(where, wq, wkv, left, right, sink_logit)
 
-    low = jnp.stack([c[96:256] for c in mine])
+    low = jnp.concatenate([c[:, 96:256] for c in mine])
     high = other_core(low)
     arriving = ring_step(low)
     state = attend(place, mine, [low, high], unroll=2)

time: 148 us -> 147 us (level)
  starting transfers between devices: 80.8 us -> 73.1 us
  waiting for transfers between devices: 25 us -> 31.6 us
    ppermute x4 -> x2, starting transfers between devices: 11.5 us -> 5.93 us  [shards(): arrived.append(lax.ppermute(chunk, ('y', 'c'), head_routes(r)))]
    ppermute x4 -> x2, waiting for transfers between devices: 3 us -> 7.73 us  [shards(): arrived.append(lax.ppermute(chunk, ('y', 'c'), head_routes(r)))]
    ppermute x15 -> x16, waiting for transfers between devices: 2.32 us -> 3.82 us  [other_core(): return lax.ppermute(value, 'c', SWAP)]
    ppermute x15 -> x16, starting transfers between devices: 12.7 us -> 13 us  [other_core(): return lax.ppermute(value, 'c', SWAP)]
  transfers between devices with their start and end apart: 36 -> 35, of which waited for: 11 -> 12; matrix products, arithmetic and copies ran while one was open for 2% -> 2% of each run, Pallas kernels for 16% -> 16%
where the time goes in v1:
time: 147 us; the launch traced here: 146 us
  starting transfers between devices  73.1 us (50%)
  Pallas kernels  36.1 us (25%)
  waiting for transfers between devices  31.6 us (21%)
  other arithmetic  3.61 us (2%)
    pallas_call x8, Pallas kernels, attend(): pl.pallas_call(functools.partial(attend_kernel, first, last, tiles, len(k...  24.8 us
    ppermute x7, starting transfers between devices, ring_step(): return lax.ppermute(value, ('z', 'c'), up + down)  21.9 us
    all_to_all x1, starting transfers between devices, shards(): back = lax.all_to_all(mixed, 'y', 0, 0, tiled=True)  16.6 us
    ppermute x7, waiting for transfers between devices, shifted(): lax.ppermute(value, axis, [(i, (i + by) % count) for i in range(count)])  15.3 us
    ppermute x16, starting transfers between devices, other_core(): return lax.ppermute(value, 'c', SWAP)  13 us
    ppermute x7, starting transfers between devices, shifted(): lax.ppermute(value, axis, [(i, (i + by) % count) for i in range(count)])  11 us
    pallas_call x1, Pallas kernels, project(): pl.pallas_call(project_kernel, out_shape=[jax.ShapeDtypeStruct((2, 256, T...  7.92 us
    ppermute x2, waiting for transfers between devices, shards(): arrived.append(lax.ppermute(chunk, ('y', 'c'), head_routes(r)))  7.73 us
  transfers between devices with their start and end apart: 35, of which 12 were waited for; matrix products, arithmetic and copies ran while one was open for 2% of the time, Pallas kernels for 16%

profile of v1, /device:TPU:1, one launch (start us, length us, event | category | flops | bytes accessed | tf_op | source)
XLA Modules:
  0.0 145.8 jit_solution(15655553196136916813)
XLA Ops:
  0.0 2.0 %collective-permute-start.1 = (bf16[512,256]{1,0:T(8,128)(2,1)}, bf16[512,256]{1,0:T(8,128)(2,1)S(1)}, u32[]{:S(2)}, u32[]{:S(2)}) collective-permute-start(bf16[512,256]{1,0:T(8,128)(2,1)} %refs_0_.1), channel_id=1, source_target_pairs={{0,2},{2,4},{4,6},{6,0},{1,3},{3,5},{5,7},{7,1},{8,10},{10,12},{12... | collective-permute-start | bytes 786440 | tf_op jit(solution)/shard_map/ppermute | solution.py:384
  3.3 4.0 %collective-permute-done.1.refs_2_ = bf16[512,256]{1,0:T(8,128)(2,1)S(1)} collective-permute-done((bf16[512,256]{1,0:T(8,128)(2,1)}, bf16[512,256]{1,0:T(8,128)(2,1)S(1)}, u32[]{:S(2)}, u32[]{:S(2)}) %collective-permute-start.1) | collective-permute-done | bytes 262176 | tf_op jit(solution)/shard_map/ppermute | solution.py:384
  7.3 2.0 %collective-permute-start.5 = (bf16[256,256]{1,0:T(8,128)(2,1)S(1)}, bf16[256,256]{1,0:T(8,128)(2,1)S(1)}, u32[]{:S(2)}, u32[]{:S(2)}) collective-permute-start(bf16[256,256]{1,0:T(8,128)(2,1)S(1)} %slice.40), channel_id=1, source_target_pairs={{0,2},{2,4},{4,6},{6,0},{1,3},{3,5},{5,7},{7,1},{8,10},{10,12},{12... | collective-permute-start | bytes 393224 | tf_op jit(solution)/shard_map/ppermute | solution.py:384
  10.9 3.5 %collective-permute-start = (bf16[512,256]{1,0:T(8,128)(2,1)}, bf16[512,256]{1,0:T(8,128)(2,1)S(1)}, u32[]{:S(2)}, u32[]{:S(2)}) collective-permute-start(bf16[512,256]{1,0:T(8,128)(2,1)} %refs_0_.1), channel_id=1, source_target_pairs={{0,1},{1,0},{2,3},{3,2},{4,5},{5,4},{6,7},{7,6},{8,9},{9,8},{10,11... | collective-permute-start | bytes 786440 | tf_op jit(solution)/shard_map/ppermute | solution.py:388
  14.9 2.3 %collective-permute-start.6 = (bf16[256,256]{1,0:T(8,128)(2,1)S(1)}, bf16[256,256]{1,0:T(8,128)(2,1)S(1)}, u32[]{:S(2)}, u32[]{:S(2)}) collective-permute-start(bf16[256,256]{1,0:T(8,128)(2,1)S(1)} %collective-permute-done.5.refs_6_), channel_id=1, source_target_pairs={{0,1},{1,0},{2,3},{3,2},{4,5},{5,4},{6,7},{7,6},{8,9},{9,8},{10,11... | collective-permute-start | bytes 393224 | tf_op jit(solution)/shard_map/ppermute | solution.py:388
  20.7 7.9 %project.1 = (bf16[2,256,256]{2,1,0:T(8,128)(2,1)}, bf16[2,256,256]{2,1,0:T(8,128)(2,1)}, bf16[4,64,256]{2,1,0:T(8,128)(2,1)}, bf16[128,512]{1,0:T(8,128)(2,1)}) custom-call(s32[4]{0:T(128)} %pad_add_fusion.place, f32[8,1,256]{2,1,0:T(1,128)} %bitcast.41, f32[1,512]{1,0:T(1,128)} %bitcast.42, f32[48,512]{1,0:T(8,128)} %get-tuple-element.77.cos_ref, ...), custom_call_target="tpu_custom_call" | custom-call | flops 2147483648 | bytes 8388608 | tf_op jit(solution)/shard_map/project/pallas_call | solution.py:160
  28.6 5.1 %collective-permute-start.9 = (bf16[2,256,256]{2,1,0:T(8,128)(2,1)}, bf16[2,256,256]{2,1,0:T(8,128)(2,1)S(1)}, u32[]{:S(2)}, u32[]{:S(2)}) collective-permute-start(bf16[2,256,256]{2,1,0:T(8,128)(2,1)} %get-tuple-element.35), channel_id=1, source_target_pairs={{0,0},{1,16},{8,8},{9,24},{16,1},{17,17},{24,9},{25,25},{2,2},{3,1... | collective-permute-start | bytes 786440 | tf_op jit(solution)/shard_map/ppermute | solution.py:457
  34.6 6.2 %collective-permute-done.9 = bf16[2,256,256]{2,1,0:T(8,128)(2,1)S(1)} collective-permute-done((bf16[2,256,256]{2,1,0:T(8,128)(2,1)}, bf16[2,256,256]{2,1,0:T(8,128)(2,1)S(1)}, u32[]{:S(2)}, u32[]{:S(2)}) %collective-permute-start.9) | collective-permute-done | bytes 262176 | tf_op jit(solution)/shard_map/ppermute | solution.py:457
  44.3 5.5 %collective-permute-start.12 = (bf16[4,160,256]{2,1,0:T(8,128)(2,1)S(1)}, bf16[4,160,256]{2,1,0:T(8,128)(2,1)S(1)}, u32[]{:S(2)}, u32[]{:S(2)}) collective-permute-start(bf16[4,160,256]{2,1,0:T(8,128)(2,1)S(1)} %pad_maximum_fusion.refs_2_), channel_id=1, source_target_pairs={{0,32},{32,64},{64,96},{96,128},{128,160},{160,192},{192,224},{224... | collective-permute-start | bytes 983048 | tf_op jit(solution)/shard_map/ppermute | solution.py:395
  51.3 2.5 %collective-permute-done.12.refs_2_ = bf16[4,160,256]{2,1,0:T(8,128)(2,1)S(1)} collective-permute-done((bf16[4,160,256]{2,1,0:T(8,128)(2,1)S(1)}, bf16[4,160,256]{2,1,0:T(8,128)(2,1)S(1)}, u32[]{:S(2)}, u32[]{:S(2)}) %collective-permute-start.12) | collective-permute-done | bytes 327712 | tf_op jit(solution)/shard_map/ppermute | solution.py:395
  53.8 3.1 %collective-permute-start.13 = (bf16[4,160,256]{2,1,0:T(8,128)(2,1)S(1)}, bf16[4,160,256]{2,1,0:T(8,128)(2,1)S(1)}, u32[]{:S(2)}, u32[]{:S(2)}) collective-permute-start(bf16[4,160,256]{2,1,0:T(8,128)(2,1)S(1)} %collective-permute-done.12.refs_2_), channel_id=1, source_target_pairs={{0,32},{32,64},{64,96},{96,128},{128,160},{160,192},{192,224},{224... | collective-permute-start | bytes 983048 | tf_op jit(solution)/shard_map/ppermute | solution.py:395
  57.4 3.1 %collective-permute-start.19 = (bf16[4,160,256]{2,1,0:T(8,128)(2,1)S(1)}, bf16[4,160,256]{2,1,0:T(8,128)(2,1)S(1)}, u32[]{:S(2)}, u32[]{:S(2)}) collective-permute-start(bf16[4,160,256]{2,1,0:T(8,128)(2,1)S(1)} %collective-permute-done.18.refs_2_), channel_id=1, source_target_pairs={{0,32},{32,64},{64,96},{96,128},{128,160},{160,192},{192,224},{224... | collective-permute-start | bytes 983048 | tf_op jit(solution)/shard_map/ppermute | solution.py:395
  61.0 3.1 %collective-permute-start.14 = (bf16[4,160,256]{2,1,0:T(8,128)(2,1)S(1)}, bf16[4,160,256]{2,1,0:T(8,128)(2,1)S(1)}, u32[]{:S(2)}, u32[]{:S(2)}) collective-permute-start(bf16[4,160,256]{2,1,0:T(8,128)(2,1)S(1)} %collective-permute-done.13.refs_2_), channel_id=1, source_target_pairs={{0,32},{32,64},{64,96},{96,128},{128,160},{160,192},{192,224},{224... | collective-permute-start | bytes 983048 | tf_op jit(solution)/shard_map/ppermute | solution.py:395
  64.7 2.9 %collective-permute-start.20 = (bf16[4,160,256]{2,1,0:T(8,128)(2,1)S(1)}, bf16[4,160,256]{2,1,0:T(8,128)(2,1)S(1)}, u32[]{:S(2)}, u32[]{:S(2)}) collective-permute-start(bf16[4,160,256]{2,1,0:T(8,128)(2,1)S(1)} %collective-permute-done.19.refs_2_), channel_id=1, source_target_pairs={{0,32},{32,64},{64,96},{96,128},{128,160},{160,192},{192,224},{224... | collective-permute-start | bytes 983048 | tf_op jit(solution)/shard_map/ppermute | solution.py:395
  67.6 3.3 %attend.7 = (f32[4,64,256]{2,1,0:T(8,128)S(1)}, f32[4,8,256]{2,1,0:T(8,128)S(1)}, f32[4,1,256]{2,1,0:T(1,128)S(1)}) custom-call(s32[4]{0:T(128)S(1)} %copy-done.1, bf16[2,256,256]{2,1,0:T(8,128)(2,1)S(1)} %pad_maximum_fusion.1.refs_0_, bf16[2,256,256]{2,1,0:T(8,128)(2,1)S(1)} %collective-permute-done.11.refs_1_, ...), custom_call_target="tpu_custom_call" | custom-call | flops 1342177280 | bytes 3145728 | tf_op jit(solution)/shard_map/attend/pallas_call | solution.py:279
  71.0 2.7 %collective-permute-start.15 = (bf16[4,160,256]{2,1,0:T(8,128)(2,1)S(1)}, bf16[4,160,256]{2,1,0:T(8,128)(2,1)S(1)}, u32[]{:S(2)}, u32[]{:S(2)}) collective-permute-start(bf16[4,160,256]{2,1,0:T(8,128)(2,1)S(1)} %collective-permute-done.14.refs_2_), channel_id=1, source_target_pairs={{0,32},{32,64},{64,96},{96,128},{128,160},{160,192},{192,224},{224... | collective-permute-start | bytes 983048 | tf_op jit(solution)/shard_map/ppermute | solution.py:395
  73.7 3.3 %attend.8 = (f32[4,64,256]{2,1,0:T(8,128)S(1)}, f32[4,8,256]{2,1,0:T(8,128)S(1)}, f32[4,1,256]{2,1,0:T(1,128)S(1)}) custom-call(s32[4]{0:T(128)S(1)} %copy-done.1, bf16[2,256,256]{2,1,0:T(8,128)(2,1)S(1)} %pad_maximum_fusion.1.refs_0_, bf16[2,256,256]{2,1,0:T(8,128)(2,1)S(1)} %collective-permute-done.11.refs_1_, ...), custom_call_target="tpu_custom_call" | custom-call | flops 1342177280 | bytes 3145728 | tf_op jit(solution)/shard_map/attend/pallas_call | solution.py:279
  77.1 3.3 %attend.9 = (f32[4,64,256]{2,1,0:T(8,128)S(1)}, f32[4,8,256]{2,1,0:T(8,128)S(1)}, f32[4,1,256]{2,1,0:T(1,128)S(1)}) custom-call(s32[4]{0:T(128)S(1)} %copy-done.1, bf16[2,256,256]{2,1,0:T(8,128)(2,1)S(1)} %pad_maximum_fusion.1.refs_0_, bf16[2,256,256]{2,1,0:T(8,128)(2,1)S(1)} %collective-permute-done.11.refs_1_, ...), custom_call_target="tpu_custom_call" | custom-call | flops 1342177280 | bytes 3145728 | tf_op jit(solution)/shard_map/attend/pallas_call | solution.py:279
  81.0 2.8 %attend.10 = (f32[4,64,256]{2,1,0:T(8,128)S(1)}, f32[4,8,256]{2,1,0:T(8,128)S(1)}, f32[4,1,256]{2,1,0:T(1,128)S(1)}) custom-call(s32[4]{0:T(128)S(1)} %copy-done.1, bf16[2,256,256]{2,1,0:T(8,128)(2,1)S(1)} %pad_maximum_fusion.1.refs_0_, bf16[2,256,256]{2,1,0:T(8,128)(2,1)S(1)} %collective-permute-done.11.refs_1_, ...), custom_call_target="tpu_custom_call" | custom-call | flops 1342177280 | bytes 3145728 | tf_op jit(solution)/shard_map/attend/pallas_call | solution.py:279
  84.2 2.8 %attend.11 = (f32[4,64,256]{2,1,0:T(8,128)S(1)}, f32[4,8,256]{2,1,0:T(8,128)S(1)}, f32[4,1,256]{2,1,0:T(1,128)S(1)}) custom-call(s32[4]{0:T(128)S(1)} %copy-done.1, bf16[2,256,256]{2,1,0:T(8,128)(2,1)S(1)} %pad_maximum_fusion.1.refs_0_, bf16[2,256,256]{2,1,0:T(8,128)(2,1)S(1)} %collective-permute-done.11.refs_1_, ...), custom_call_target="tpu_custom_call" | custom-call | flops 1342177280 | bytes 3145728 | tf_op jit(solution)/shard_map/attend/pallas_call | solution.py:279
  87.0 2.8 %attend.12 = (f32[4,64,256]{2,1,0:T(8,128)S(1)}, f32[4,8,256]{2,1,0:T(8,128)S(1)}, f32[4,1,256]{2,1,0:T(1,128)S(1)}) custom-call(s32[4]{0:T(128)S(1)} %copy-done.1, bf16[2,256,256]{2,1,0:T(8,128)(2,1)S(1)} %pad_maximum_fusion.1.refs_0_, bf16[2,256,256]{2,1,0:T(8,128)(2,1)S(1)} %collective-permute-done.11.refs_1_, ...), custom_call_target="tpu_custom_call" | custom-call | flops 1342177280 | bytes 3145728 | tf_op jit(solution)/shard_map/attend/pallas_call | solution.py:279
  89.9 2.8 %attend.13 = (f32[4,64,256]{2,1,0:T(8,128)S(1)}, f32[4,8,256]{2,1,0:T(8,128)S(1)}, f32[4,1,256]{2,1,0:T(1,128)S(1)}) custom-call(s32[4]{0:T(128)S(1)} %copy-done.1, bf16[2,256,256]{2,1,0:T(8,128)(2,1)S(1)} %pad_maximum_fusion.1.refs_0_, bf16[2,256,256]{2,1,0:T(8,128)(2,1)S(1)} %collective-permute-done.11.refs_1_, ...), custom_call_target="tpu_custom_call" | custom-call | flops 1342177280 | bytes 3145728 | tf_op jit(solution)/shard_map/attend/pallas_call | solution.py:279
  92.8 3.5 %attend_last.1 = bf16[4,64,256]{2,1,0:T(8,128)(2,1)} custom-call(s32[4]{0:T(128)S(1)} %copy-done.1, bf16[2,256,256]{2,1,0:T(8,128)(2,1)S(1)} %pad_maximum_fusion.1.refs_0_, bf16[2,256,256]{2,1,0:T(8,128)(2,1)S(1)} %collective-permute-done.11.refs_1_, bf16[4,160,256]{2,1,0:T(8,128)(2,1)S(1)} %collective-permute-done.15.refs_2_, ...), custom_call_target="tpu_custom_call" | custom-call | flops 1342177280 | bytes 3145728 | tf_op jit(solution)/shard_map/attend_last/pallas_call | solution.py:279
  96.4 16.6 %all-to-all-start = ((bf16[4,64,256]{2,1,0:T(8,128)(2,1)}), bf16[4,64,256]{2,1,0:T(8,128)(2,1)S(1)}, u32[]{:S(2)}, u32[]{:S(2)}) async-start(bf16[4,64,256]{2,1,0:T(8,128)(2,1)} %attend_last.1), calls=%async_computation | async-start | bytes 262144 | tf_op jit(solution)/shard_map/all_to_all | solution.py:491
  113.0 3.4 %collective-permute-start.28 = (bf16[128,128]{1,0:T(8,128)(2,1)S(1)}, bf16[128,128]{1,0:T(8,128)(2,1)S(1)}, u32[]{:S(2)}, u32[]{:S(2)}) collective-permute-start(bf16[128,128]{1,0:T(8,128)(2,1)S(1)} %get-tuple-element.73), channel_id=1, source_target_pairs={{0,8},{8,16},{16,24},{24,32},{32,40},{40,48},{48,56},{56,64},{64,7... | collective-permute-start | bytes 98312 | tf_op jit(solution)/shard_map/ppermute | solution.py:461
  117.8 2.0 %collective-permute-start.27 = (bf16[2,64,256]{2,1,0:T(8,128)(2,1)S(1)}, bf16[2,64,256]{2,1,0:T(8,128)(2,1)S(1)}, u32[]{:S(2)}, u32[]{:S(2)}) collective-permute-start(bf16[2,64,256]{2,1,0:T(8,128)(2,1)S(1)} %get-tuple-element.74), channel_id=1, source_target_pairs={{0,1},{1,0},{2,3},{3,2},{4,5},{5,4},{6,7},{7,6},{8,9},{9,8},{10,11... | collective-permute-start | bytes 196616 | tf_op jit(solution)/shard_map/ppermute | solution.py:388
  121.0 2.0 %windowed.1.win_ref = bf16[128,512]{1,0:T(8,128)(2,1)S(1)} custom-call(s32[2]{0:T(128)S(1)} %pad_add_fusion.1.span_ref, bf16[4,64,256]{2,1,0:T(8,128)(2,1)S(1)} %copy-done.5, bf16[128,512]{1,0:T(8,128)(2,1)S(1)} %copy-done, bf16[128,128]{1,0:T(8,128)(2,1)S(1)} %collective-permute-done.28.left_ref, bf16[128,128]{1,0:T(8,128)(2,1)S(1)} %collective-permute-done.29.right_ref, ...), custom_call_target="tpu_custom_call" | custom-call | flops 100663296 | bytes 1048576 | tf_op jit(solution)/shard_map/windowed/pallas_call | solution.py:328
  124.4 2.5 %collective-permute-start.30 = (bf16[4,512,256]{2,1,0:T(8,128)(2,1)S(1)}, bf16[4,512,256]{2,1,0:T(8,128)(2,1)S(1)}, u32[]{:S(2)}, u32[]{:S(2)}) collective-permute-start(bf16[4,512,256]{2,1,0:T(8,128)(2,1)S(1)} %get-tuple-element.61), channel_id=1, source_target_pairs={{0,1},{1,0},{2,3},{3,2},{4,5},{5,4},{6,7},{7,6},{8,9},{9,8},{10,11... | collective-permute-start | bytes 3145736 | tf_op jit(solution)/shard_map/ppermute | solution.py:388
  127.0 2.3 %collective-permute-done.30 = bf16[4,512,256]{2,1,0:T(8,128)(2,1)S(1)} collective-permute-done((bf16[4,512,256]{2,1,0:T(8,128)(2,1)S(1)}, bf16[4,512,256]{2,1,0:T(8,128)(2,1)S(1)}, u32[]{:S(2)}, u32[]{:S(2)}) %collective-permute-start.30) | collective-permute-done | bytes 1048608 | tf_op jit(solution)/shard_map/ppermute | solution.py:388
  131.5 2.0 %collective-permute-start.33 = (bf16[512,256]{1,0:T(8,128)(2,1)S(1)}, bf16[512,256]{1,0:T(8,128)(2,1)S(1)}, u32[]{:S(2)}, u32[]{:S(2)}) collective-permute-start(bf16[512,256]{1,0:T(8,128)(2,1)S(1)} %get-tuple-element.66), channel_id=1, source_target_pairs={{0,6},{2,0},{4,2},{6,4},{1,7},{3,1},{5,3},{7,5},{8,14},{10,8},{12,... | collective-permute-start | bytes 786440 | tf_op jit(solution)/shard_map/ppermute | solution.py:384
  133.6 5.0 %collective-permute-done.31 = bf16[512,256]{1,0:T(8,128)(2,1)S(1)} collective-permute-done((bf16[512,256]{1,0:T(8,128)(2,1)S(1)}, bf16[512,256]{1,0:T(8,128)(2,1)S(1)}, u32[]{:S(2)}, u32[]{:S(2)}) %collective-permute-start.31) | collective-permute-done | bytes 262176 | tf_op jit(solution)/shard_map/ppermute | solution.py:384
  138.6 6.3 %collective-permute-done.32 = bf16[512,256]{1,0:T(8,128)(2,1)S(1)} collective-permute-done((bf16[512,256]{1,0:T(8,128)(2,1)S(1)}, bf16[512,256]{1,0:T(8,128)(2,1)S(1)}, u32[]{:S(2)}, u32[]{:S(2)}) %collective-permute-start.32) | collective-permute-done | bytes 262176 | tf_op jit(solution)/shard_map/ppermute | solution.py:384
  (96 shorter events, 22.3 us)
Async XLA Ops:
  0.0 7.3 %collective-permute-start.1 = (bf16[512,256]{1,0:T(8,128)(2,1)}, bf16[512,256]{1,0:T(8,128)(2,1)S(1)}, u32[]{:S(2)}, u32[]{:S(2)}) collective-permute-start(bf16[512,256]{1,0:T(8,128)(2,1)} %refs_0_.1), channel_id=1, source_target_pairs={{0,2},{2,4},{4,6},{6,0},{1,3},{3,5},{5,7},{7,1},{8,10},{10,12},{12... | collective-permute-start | bytes 786440 | tf_op jit(solution)/shard_map/ppermute | solution.py:384
  2.0 7.3 %collective-permute-start.3 = (bf16[512,256]{1,0:T(8,128)(2,1)}, bf16[512,256]{1,0:T(8,128)(2,1)S(1)}, u32[]{:S(2)}, u32[]{:S(2)}) collective-permute-start(bf16[512,256]{1,0:T(8,128)(2,1)} %refs_0_.1), channel_id=1, source_target_pairs={{0,6},{2,0},{4,2},{6,4},{1,7},{3,1},{5,3},{7,5},{8,14},{10,8},{12,... | collective-permute-start | bytes 786440 | tf_op jit(solution)/shard_map/ppermute | solution.py:384
  7.3 7.7 %collective-permute-start.5 = (bf16[256,256]{1,0:T(8,128)(2,1)S(1)}, bf16[256,256]{1,0:T(8,128)(2,1)S(1)}, u32[]{:S(2)}, u32[]{:S(2)}) collective-permute-start(bf16[256,256]{1,0:T(8,128)(2,1)S(1)} %slice.40), channel_id=1, source_target_pairs={{0,2},{2,4},{4,6},{6,0},{1,3},{3,5},{5,7},{7,1},{8,10},{10,12},{12... | collective-permute-start | bytes 393224 | tf_op jit(solution)/shard_map/ppermute | solution.py:384
  9.3 7.9 %collective-permute-start.7 = (bf16[256,256]{1,0:T(8,128)(2,1)S(1)}, bf16[256,256]{1,0:T(8,128)(2,1)S(1)}, u32[]{:S(2)}, u32[]{:S(2)}) collective-permute-start(bf16[256,256]{1,0:T(8,128)(2,1)S(1)} %slice.41), channel_id=1, source_target_pairs={{0,6},{2,0},{4,2},{6,4},{1,7},{3,1},{5,3},{7,5},{8,14},{10,8},{12,... | collective-permute-start | bytes 393224 | tf_op jit(solution)/shard_map/ppermute | solution.py:384
  10.9 8.8 %collective-permute-start = (bf16[512,256]{1,0:T(8,128)(2,1)}, bf16[512,256]{1,0:T(8,128)(2,1)S(1)}, u32[]{:S(2)}, u32[]{:S(2)}) collective-permute-start(bf16[512,256]{1,0:T(8,128)(2,1)} %refs_0_.1), channel_id=1, source_target_pairs={{0,1},{1,0},{2,3},{3,2},{4,5},{5,4},{6,7},{7,6},{8,9},{9,8},{10,11... | collective-permute-start | bytes 786440 | tf_op jit(solution)/shard_map/ppermute | solution.py:388
  14.4 5.3 %collective-permute-start.2 = (bf16[512,256]{1,0:T(8,128)(2,1)S(1)}, bf16[512,256]{1,0:T(8,128)(2,1)S(1)}, u32[]{:S(2)}, u32[]{:S(2)}) collective-permute-start(bf16[512,256]{1,0:T(8,128)(2,1)S(1)} %collective-permute-done.1.refs_2_), channel_id=1, source_target_pairs={{0,1},{1,0},{2,3},{3,2},{4,5},{5,4},{6,7},{7,6},{8,9},{9,8},{10,11... | collective-permute-start | bytes 786440 | tf_op jit(solution)/shard_map/ppermute | solution.py:388
  14.4 5.4 %collective-permute-start.4 = (bf16[512,256]{1,0:T(8,128)(2,1)S(1)}, bf16[512,256]{1,0:T(8,128)(2,1)S(1)}, u32[]{:S(2)}, u32[]{:S(2)}) collective-permute-start(bf16[512,256]{1,0:T(8,128)(2,1)S(1)} %collective-permute-done.3.refs_4_), channel_id=1, source_target_pairs={{0,1},{1,0},{2,3},{3,2},{4,5},{5,4},{6,7},{7,6},{8,9},{9,8},{10,11... | collective-permute-start | bytes 786440 | tf_op jit(solution)/shard_map/ppermute | solution.py:388
  14.9 4.8 %collective-permute-start.6 = (bf16[256,256]{1,0:T(8,128)(2,1)S(1)}, bf16[256,256]{1,0:T(8,128)(2,1)S(1)}, u32[]{:S(2)}, u32[]{:S(2)}) collective-permute-start(bf16[256,256]{1,0:T(8,128)(2,1)S(1)} %collective-permute-done.5.refs_6_), channel_id=1, source_target_pairs={{0,1},{1,0},{2,3},{3,2},{4,5},{5,4},{6,7},{7,6},{8,9},{9,8},{10,11... | collective-permute-start | bytes 393224 | tf_op jit(solution)/shard_map/ppermute | solution.py:388
  28.6 12.2 %collective-permute-start.9 = (bf16[2,256,256]{2,1,0:T(8,128)(2,1)}, bf16[2,256,256]{2,1,0:T(8,128)(2,1)S(1)}, u32[]{:S(2)}, u32[]{:S(2)}) collective-permute-start(bf16[2,256,256]{2,1,0:T(8,128)(2,1)} %get-tuple-element.35), channel_id=1, source_target_pairs={{0,0},{1,16},{8,8},{9,24},{16,1},{17,17},{24,9},{25,25},{2,2},{3,1... | collective-permute-start | bytes 786440 | tf_op jit(solution)/shard_map/ppermute | solution.py:457
  33.7 8.6 %collective-permute-start.10 = (bf16[2,256,256]{2,1,0:T(8,128)(2,1)}, bf16[2,256,256]{2,1,0:T(8,128)(2,1)S(1)}, u32[]{:S(2)}, u32[]{:S(2)}) collective-permute-start(bf16[2,256,256]{2,1,0:T(8,128)(2,1)} %get-tuple-element.36), channel_id=1, source_target_pairs={{0,8},{1,24},{8,0},{9,16},{16,9},{17,25},{24,1},{25,17},{2,10},{3,... | collective-permute-start | bytes 786440 | tf_op jit(solution)/shard_map/ppermute | solution.py:457
  44.1 5.8 %collective-permute-start.17 = (bf16[4,160,256]{2,1,0:T(8,128)(2,1)S(1)}, bf16[4,160,256]{2,1,0:T(8,128)(2,1)S(1)}, u32[]{:S(2)}, u32[]{:S(2)}) collective-permute-start(bf16[4,160,256]{2,1,0:T(8,128)(2,1)S(1)} %pad_maximum_fusion.refs_2_), channel_id=1, source_target_pairs={{0,1},{1,0},{2,3},{3,2},{4,5},{5,4},{6,7},{7,6},{8,9},{9,8},{10,11... | collective-permute-start | bytes 983048 | tf_op jit(solution)/shard_map/ppermute | solution.py:388
  44.3 9.6 %collective-permute-start.12 = (bf16[4,160,256]{2,1,0:T(8,128)(2,1)S(1)}, bf16[4,160,256]{2,1,0:T(8,128)(2,1)S(1)}, u32[]{:S(2)}, u32[]{:S(2)}) collective-permute-start(bf16[4,160,256]{2,1,0:T(8,128)(2,1)S(1)} %pad_maximum_fusion.refs_2_), channel_id=1, source_target_pairs={{0,32},{32,64},{64,96},{96,128},{128,160},{160,192},{192,224},{224... | collective-permute-start | bytes 983048 | tf_op jit(solution)/shard_map/ppermute | solution.py:395
  49.8 7.5 %collective-permute-start.18 = (bf16[4,160,256]{2,1,0:T(8,128)(2,1)S(1)}, bf16[4,160,256]{2,1,0:T(8,128)(2,1)S(1)}, u32[]{:S(2)}, u32[]{:S(2)}) collective-permute-start(bf16[4,160,256]{2,1,0:T(8,128)(2,1)S(1)} %collective-permute-done.17.refs_3_), channel_id=1, source_target_pairs={{0,32},{32,64},{64,96},{96,128},{128,160},{160,192},{192,224},{224... | collective-permute-start | bytes 983048 | tf_op jit(solution)/shard_map/ppermute | solution.py:395
  53.8 7.1 %collective-permute-start.13 = (bf16[4,160,256]{2,1,0:T(8,128)(2,1)S(1)}, bf16[4,160,256]{2,1,0:T(8,128)(2,1)S(1)}, u32[]{:S(2)}, u32[]{:S(2)}) collective-permute-start(bf16[4,160,256]{2,1,0:T(8,128)(2,1)S(1)} %collective-permute-done.12.refs_2_), channel_id=1, source_target_pairs={{0,32},{32,64},{64,96},{96,128},{128,160},{160,192},{192,224},{224... | collective-permute-start | bytes 983048 | tf_op jit(solution)/shard_map/ppermute | solution.py:395
  57.4 7.4 %collective-permute-start.19 = (bf16[4,160,256]{2,1,0:T(8,128)(2,1)S(1)}, bf16[4,160,256]{2,1,0:T(8,128)(2,1)S(1)}, u32[]{:S(2)}, u32[]{:S(2)}) collective-permute-start(bf16[4,160,256]{2,1,0:T(8,128)(2,1)S(1)} %collective-permute-done.18.refs_2_), channel_id=1, source_target_pairs={{0,32},{32,64},{64,96},{96,128},{128,160},{160,192},{192,224},{224... | collective-permute-start | bytes 983048 | tf_op jit(solution)/shard_map/ppermute | solution.py:395
  60.5 10.5 %collective-permute-start.26 = (bf16[4,160,256]{2,1,0:T(8,128)(2,1)S(1)}, bf16[4,160,256]{2,1,0:T(8,128)(2,1)S(1)}, u32[]{:S(2)}, u32[]{:S(2)}) collective-permute-start(bf16[4,160,256]{2,1,0:T(8,128)(2,1)S(1)} %collective-permute-done.12.refs_2_), channel_id=1, source_target_pairs={{0,1},{1,0},{2,3},{3,2},{4,5},{5,4},{6,7},{7,6},{8,9},{9,8},{10,11... | collective-permute-start | bytes 983048 | tf_op jit(solution)/shard_map/ppermute | solution.py:388
  61.0 10.1 %collective-permute-start.14 = (bf16[4,160,256]{2,1,0:T(8,128)(2,1)S(1)}, bf16[4,160,256]{2,1,0:T(8,128)(2,1)S(1)}, u32[]{:S(2)}, u32[]{:S(2)}) collective-permute-start(bf16[4,160,256]{2,1,0:T(8,128)(2,1)S(1)} %collective-permute-done.13.refs_2_), channel_id=1, source_target_pairs={{0,32},{32,64},{64,96},{96,128},{128,160},{160,192},{192,224},{224... | collective-permute-start | bytes 983048 | tf_op jit(solution)/shard_map/ppermute | solution.py:395
  64.1 12.9 %collective-permute-start.25 = (bf16[4,160,256]{2,1,0:T(8,128)(2,1)S(1)}, bf16[4,160,256]{2,1,0:T(8,128)(2,1)S(1)}, u32[]{:S(2)}, u32[]{:S(2)}) collective-permute-start(bf16[4,160,256]{2,1,0:T(8,128)(2,1)S(1)} %collective-permute-done.18.refs_2_), channel_id=1, source_target_pairs={{0,1},{1,0},{2,3},{3,2},{4,5},{5,4},{6,7},{7,6},{8,9},{9,8},{10,11... | collective-permute-start | bytes 983048 | tf_op jit(solution)/shard_map/ppermute | solution.py:388
  64.1 16.9 %collective-permute-start.24 = (bf16[4,160,256]{2,1,0:T(8,128)(2,1)S(1)}, bf16[4,160,256]{2,1,0:T(8,128)(2,1)S(1)}, u32[]{:S(2)}, u32[]{:S(2)}) collective-permute-start(bf16[4,160,256]{2,1,0:T(8,128)(2,1)S(1)} %collective-permute-done.13.refs_2_), channel_id=1, source_target_pairs={{0,1},{1,0},{2,3},{3,2},{4,5},{5,4},{6,7},{7,6},{8,9},{9,8},{10,11... | collective-permute-start | bytes 983048 | tf_op jit(solution)/shard_map/ppermute | solution.py:388
  64.7 15.7 %collective-permute-start.20 = (bf16[4,160,256]{2,1,0:T(8,128)(2,1)S(1)}, bf16[4,160,256]{2,1,0:T(8,128)(2,1)S(1)}, u32[]{:S(2)}, u32[]{:S(2)}) collective-permute-start(bf16[4,160,256]{2,1,0:T(8,128)(2,1)S(1)} %collective-permute-done.19.refs_2_), channel_id=1, source_target_pairs={{0,32},{32,64},{64,96},{96,128},{128,160},{160,192},{192,224},{224... | collective-permute-start | bytes 983048 | tf_op jit(solution)/shard_map/ppermute | solution.py:395
  70.9 13.2 %collective-permute-start.23 = (bf16[4,160,256]{2,1,0:T(8,128)(2,1)S(1)}, bf16[4,160,256]{2,1,0:T(8,128)(2,1)S(1)}, u32[]{:S(2)}, u32[]{:S(2)}) collective-permute-start(bf16[4,160,256]{2,1,0:T(8,128)(2,1)S(1)} %collective-permute-done.19.refs_2_), channel_id=1, source_target_pairs={{0,1},{1,0},{2,3},{3,2},{4,5},{5,4},{6,7},{7,6},{8,9},{9,8},{10,11... | collective-permute-start | bytes 983048 | tf_op jit(solution)/shard_map/ppermute | solution.py:388
  71.0 12.8 %collective-permute-start.15 = (bf16[4,160,256]{2,1,0:T(8,128)(2,1)S(1)}, bf16[4,160,256]{2,1,0:T(8,128)(2,1)S(1)}, u32[]{:S(2)}, u32[]{:S(2)}) collective-permute-start(bf16[4,160,256]{2,1,0:T(8,128)(2,1)S(1)} %collective-permute-done.14.refs_2_), channel_id=1, source_target_pairs={{0,32},{32,64},{64,96},{96,128},{128,160},{160,192},{192,224},{224... | collective-permute-start | bytes 983048 | tf_op jit(solution)/shard_map/ppermute | solution.py:395
  77.0 10.0 %collective-permute-start.22 = (bf16[4,160,256]{2,1,0:T(8,128)(2,1)S(1)}, bf16[4,160,256]{2,1,0:T(8,128)(2,1)S(1)}, u32[]{:S(2)}, u32[]{:S(2)}) collective-permute-start(bf16[4,160,256]{2,1,0:T(8,128)(2,1)S(1)} %collective-permute-done.14.refs_2_), channel_id=1, source_target_pairs={{0,1},{1,0},{2,3},{3,2},{4,5},{5,4},{6,7},{7,6},{8,9},{9,8},{10,11... | collective-permute-start | bytes 983048 | tf_op jit(solution)/shard_map/ppermute | solution.py:388
  80.4 9.5 %collective-permute-start.21 = (bf16[4,160,256]{2,1,0:T(8,128)(2,1)S(1)}, bf16[4,160,256]{2,1,0:T(8,128)(2,1)S(1)}, u32[]{:S(2)}, u32[]{:S(2)}) collective-permute-start(bf16[4,160,256]{2,1,0:T(8,128)(2,1)S(1)} %collective-permute-done.20.refs_2_), channel_id=1, source_target_pairs={{0,1},{1,0},{2,3},{3,2},{4,5},{5,4},{6,7},{7,6},{8,9},{9,8},{10,11... | collective-permute-start | bytes 983048 | tf_op jit(solution)/shard_map/ppermute | solution.py:388
  83.8 8.9 %collective-permute-start.16 = (bf16[4,160,256]{2,1,0:T(8,128)(2,1)S(1)}, bf16[4,160,256]{2,1,0:T(8,128)(2,1)S(1)}, u32[]{:S(2)}, u32[]{:S(2)}) collective-permute-start(bf16[4,160,256]{2,1,0:T(8,128)(2,1)S(1)} %collective-permute-done.15.refs_2_), channel_id=1, source_target_pairs={{0,1},{1,0},{2,3},{3,2},{4,5},{5,4},{6,7},{7,6},{8,9},{9,8},{10,11... | collective-permute-start | bytes 983048 | tf_op jit(solution)/shard_map/ppermute | solution.py:388
  96.4 21.4 %all-to-all-start = ((bf16[4,64,256]{2,1,0:T(8,128)(2,1)}), bf16[4,64,256]{2,1,0:T(8,128)(2,1)S(1)}, u32[]{:S(2)}, u32[]{:S(2)}) async-start(bf16[4,64,256]{2,1,0:T(8,128)(2,1)} %attend_last.1), calls=%async_computation | async-start | bytes 262144 | tf_op jit(solution)/shard_map/all_to_all | solution.py:491
  113.0 6.9 %collective-permute-start.28 = (bf16[128,128]{1,0:T(8,128)(2,1)S(1)}, bf16[128,128]{1,0:T(8,128)(2,1)S(1)}, u32[]{:S(2)}, u32[]{:S(2)}) collective-permute-start(bf16[128,128]{1,0:T(8,128)(2,1)S(1)} %get-tuple-element.73), channel_id=1, source_target_pairs={{0,8},{8,16},{16,24},{24,32},{32,40},{40,48},{48,56},{56,64},{64,7... | collective-permute-start | bytes 98312 | tf_op jit(solution)/shard_map/ppermute | solution.py:461
  117.8 5.3 %collective-permute-start.27 = (bf16[2,64,256]{2,1,0:T(8,128)(2,1)S(1)}, bf16[2,64,256]{2,1,0:T(8,128)(2,1)S(1)}, u32[]{:S(2)}, u32[]{:S(2)}) collective-permute-start(bf16[2,64,256]{2,1,0:T(8,128)(2,1)S(1)} %get-tuple-element.74), channel_id=1, source_target_pairs={{0,1},{1,0},{2,3},{3,2},{4,5},{5,4},{6,7},{7,6},{8,9},{9,8},{10,11... | collective-permute-start | bytes 196616 | tf_op jit(solution)/shard_map/ppermute | solution.py:388
  124.4 4.8 %collective-permute-start.30 = (bf16[4,512,256]{2,1,0:T(8,128)(2,1)S(1)}, bf16[4,512,256]{2,1,0:T(8,128)(2,1)S(1)}, u32[]{:S(2)}, u32[]{:S(2)}) collective-permute-start(bf16[4,512,256]{2,1,0:T(8,128)(2,1)S(1)} %get-tuple-element.61), channel_id=1, source_target_pairs={{0,1},{1,0},{2,3},{3,2},{4,5},{5,4},{6,7},{7,6},{8,9},{9,8},{10,11... | collective-permute-start | bytes 3145736 | tf_op jit(solution)/shard_map/ppermute | solution.py:388
  129.5 9.1 %collective-permute-start.31 = (bf16[512,256]{1,0:T(8,128)(2,1)S(1)}, bf16[512,256]{1,0:T(8,128)(2,1)S(1)}, u32[]{:S(2)}, u32[]{:S(2)}) collective-permute-start(bf16[512,256]{1,0:T(8,128)(2,1)S(1)} %get-tuple-element.65), channel_id=1, source_target_pairs={{0,4},{2,6},{4,0},{6,2},{1,5},{3,7},{5,1},{7,3},{8,12},{10,14},{12... | collective-permute-start | bytes 786440 | tf_op jit(solution)/shard_map/ppermute | solution.py:384
  130.9 14.0 %collective-permute-start.32 = (bf16[512,256]{1,0:T(8,128)(2,1)S(1)}, bf16[512,256]{1,0:T(8,128)(2,1)S(1)}, u32[]{:S(2)}, u32[]{:S(2)}) collective-permute-start(bf16[512,256]{1,0:T(8,128)(2,1)S(1)} %get-tuple-element.67), channel_id=1, source_target_pairs={{0,2},{2,4},{4,6},{6,0},{1,3},{3,5},{5,7},{7,1},{8,10},{10,12},{12... | collective-permute-start | bytes 786440 | tf_op jit(solution)/shard_map/ppermute | solution.py:384
  131.5 13.4 %collective-permute-start.33 = (bf16[512,256]{1,0:T(8,128)(2,1)S(1)}, bf16[512,256]{1,0:T(8,128)(2,1)S(1)}, u32[]{:S(2)}, u32[]{:S(2)}) collective-permute-start(bf16[512,256]{1,0:T(8,128)(2,1)S(1)} %get-tuple-element.66), channel_id=1, source_target_pairs={{0,6},{2,0},{4,2},{6,4},{1,7},{3,1},{5,3},{7,5},{8,14},{10,8},{12,... | collective-permute-start | bytes 786440 | tf_op jit(solution)/shard_map/ppermute | solution.py:384
  (18 other events, 219.6 us)
